TPU v7x, 32 devices: a whole 2x2x4 slice. The times are simulated.
32 devices in a mesh: grp: 2 (over x), tp: 16 (over z, y, core).
Axes of the slice: x: 2, y: 2, z: 4, core: 2. Of those that a mesh axis runs over, the one named last changes fastest.
Arguments:
- tokens: bfloat16 [128, 2048], P('grp'), parts along dimension 0, may hold values from -6 to 6
- norm_gain: float32 [2, 2048], replicated, may hold values from 0.1 to 1.9
- query_weight: bfloat16 [2, 2048, 2048], P(None, 'tp'), may hold values from -0.125 to 0.125
- key_weight: bfloat16 [2, 2048, 2048], P(None, 'tp'), may hold values from -0.125 to 0.125
- value_weight: bfloat16 [2, 2048, 2048], P(None, 'tp'), may hold values from -0.125 to 0.125
- outgate_weight: bfloat16 [2, 2048, 2048], P(None, 'tp'), may hold values from -0.125 to 0.125
- gate_weight: bfloat16 [2, 2048, 16], replicated, may hold values from -0.125 to 0.125
- forget_bias: float32 [2, 8], replicated, may hold values from 0 to 4
- proj_weight: bfloat16 [2, 2048, 2048], P(None, 'tp'), may hold values from -0.125 to 0.125
- cell_state: float32 [2, 128, 2048, 256], P(None, 'grp', 'tp'), parts along dimension 1, may hold values from -0.3 to 0.3
- normalizer: float32 [2, 128, 2048], P(None, 'grp', 'tp'), parts along dimension 1, may hold values from -0.3 to 0.3
- stabilizer: float32 [2, 128, 8], P(None, 'grp'), parts along dimension 1, may hold values from -2 to 2
Outputs:
- mixed: bfloat16 [128, 2048], P('grp', 'tp'), parts along dimension 0
- new_cell: float32 [2, 128, 2048, 256], P(None, 'grp', 'tp'), parts along dimension 1
- new_normalizer: float32 [2, 128, 2048], P(None, 'grp', 'tp'), parts along dimension 1
- new_stabilizer: float32 [2, 128, 8], P(None, 'grp'), parts along dimension 1
There are 2 independent parts, one for each index of `grp`. A program takes and returns all parts, laid end to end along the dimension named above; an argument that names none is the same for every part. Nothing has to cross between parts.
All inputs are finite; a program needn't handle non-finite values.
Results may differ from a plain program's by a relative error of at most 0.025.
Values may be sent and summed in bfloat16 or wider, within the bound.
A program may use at most 64 MiB of HBM per device.

v0:
```python
import functools

import jax
import jax.numpy as jnp
from jax import lax
from jax.experimental import pallas as pl
from jax.experimental.pallas import tpu as pltpu
from jax.sharding import PartitionSpec as P

D = 2048
DH = 256
LAYERS = 2


epsilon = 1e-06


def from_partner(value, axis, apart):
    mask = 2**apart
    pairs = [(source, source ^ mask) for source in range(lax.axis_size(axis))]
    return lax.ppermute(value, axis, pairs)


def project(normed, weight):
    return lax.dot_general(
        normed, weight, (((1,), (1,)), ((), ())), preferred_element_type=jnp.float32
    )


def split_pieces(value):
    high = lax.optimization_barrier(value.astype(jnp.bfloat16))
    rest = value - high.astype(jnp.float32)
    middle = lax.optimization_barrier(rest.astype(jnp.bfloat16))
    lowest = (rest - middle.astype(jnp.float32)).astype(jnp.bfloat16)
    return jnp.stack([high, middle, lowest], axis=1)


def join_pieces(pieces):
    return jnp.sum(pieces.astype(jnp.float32), axis=-1)


def combine_halves(mine, theirs, lower):
    return jnp.where(
        lower, jnp.concatenate([mine, theirs], axis=1), jnp.concatenate([theirs, mine], axis=1)
    )


def one_cell(
    current,
    gain,
    w_query,
    w_key,
    w_value,
    w_outgate,
    w_gates,
    bias_forget,
    w_proj,
    cell,
    norm_vec,
    stab,
):
    heads = D // DH
    ncols = w_query.shape[0]
    group = DH // ncols
    device = lax.axis_index("tp")
    head = device // group
    cur_f = current.astype(jnp.float32)
    normed = (
        cur_f * lax.rsqrt(jnp.mean(cur_f * cur_f, axis=-1, keepdims=True) + epsilon) * gain
    ).astype(jnp.bfloat16)
    query = project(normed, w_query).astype(jnp.bfloat16)
    keys = (project(normed, w_key) * DH ** (-0.5)).astype(jnp.bfloat16)
    values = project(normed, w_value).astype(jnp.bfloat16)
    outgate = project(normed, w_outgate).astype(jnp.bfloat16)
    gates = jnp.dot(normed, w_gates, preferred_element_type=jnp.float32)
    in_gate = gates[:, :heads]
    log_forget = jax.nn.log_sigmoid(gates[:, heads:] + bias_forget)
    new_stab = jnp.maximum(log_forget + stab, in_gate)
    decay = jnp.exp(log_forget + stab - new_stab)
    weight_in = jnp.exp(in_gate - new_stab)
    select = (jnp.arange(heads) == head).astype(jnp.float32)
    my_decay = jnp.sum(decay * select, axis=-1)
    my_weight = jnp.sum(weight_in * select, axis=-1)
    my_stab = jnp.sum(new_stab * select, axis=-1)
    new_norm = my_decay[:, None] * norm_vec + my_weight[:, None] * keys.astype(jnp.float32)
    den_part = jnp.sum(query.astype(jnp.float32) * new_norm, axis=-1)
    q_head, k_head = (query, keys)
    denom = den_part
    for bit in range(group.bit_length() - 1):
        other_q, other_k, other_pieces = from_partner(
            (q_head, k_head, split_pieces(denom)), "tp", bit
        )
        lower = device // 2**bit % 2 == 0
        q_head = combine_halves(q_head, other_q, lower)
        k_head = combine_halves(k_head, other_k, lower)
        denom = denom + join_pieces(other_pieces)
    outer = values.astype(jnp.float32)[:, :, None] * k_head.astype(jnp.float32)[:, None, :]
    new_cell = my_decay[:, None, None] * cell + my_weight[:, None, None] * outer
    numer = jnp.einsum(
        "bk,bek->be", q_head.astype(jnp.float32), new_cell, precision=lax.Precision.HIGHEST
    )
    readout = numer / jnp.maximum(jnp.abs(denom), jnp.exp(-my_stab))[:, None]
    branch = (jax.nn.sigmoid(outgate.astype(jnp.float32)) * readout).astype(jnp.bfloat16)
    summed = project(lax.all_gather(branch, "tp", axis=1, tiled=True), w_proj)
    own_input = lax.dynamic_slice_in_dim(cur_f, device * ncols, ncols, 1)
    result = (own_input + summed).astype(jnp.bfloat16)
    return (result, new_cell, new_norm, new_stab)


def body(
    tokens,
    norm_gain,
    query_weight,
    key_weight,
    value_weight,
    outgate_weight,
    gate_weight,
    forget_bias,
    proj_weight,
    cell_state,
    normalizer,
    stabilizer,
):
    current = tokens
    cells = []
    norms = []
    stabs = []
    result = tokens
    for layer in range(LAYERS):
        result, new_cell, new_norm, new_stab = one_cell(
            current,
            norm_gain[layer],
            query_weight[layer],
            key_weight[layer],
            value_weight[layer],
            outgate_weight[layer],
            gate_weight[layer],
            forget_bias[layer],
            proj_weight[layer],
            cell_state[layer],
            normalizer[layer],
            stabilizer[layer],
        )
        cells.append(new_cell)
        norms.append(new_norm)
        stabs.append(new_stab)
        if layer + 1 < LAYERS:
            current = lax.all_gather(result, "tp", axis=1, tiled=True)
    return (result, jnp.stack(cells), jnp.stack(norms), jnp.stack(stabs))


NT = (((1,), (1,)), ((), ()))
CELL_CHUNKS = 4


def fused_kernel(
    n,
    group,
    tokens,
    norm_gain,
    w_query,
    w_key,
    w_value,
    w_outgate,
    w_gates,
    bias_forget,
    w_proj,
    cell,
    norm_vec,
    stab,
    mixed,
    cell_buf,
    new_norm,
    new_stab,
    wv_buf,
    key_buf,
    decay_buf,
    tok_buf,
    gain_buf,
    weights,
    gate_buf,
    bias_buf,
    stab_buf,
    norm_buf,
    pair_buf,
    branch_buf,
    result_buf,
    numer_buf,
    small_sem,
    weight_sem,
    cell_sem,
    norm_send,
    norm_recv,
    pair_send,
    pair_recv,
    gather_send,
    gather_recv,
):
    layers, batch, ncols, dh = cell.shape
    width = tokens.shape[1]
    heads = stab.shape[1]
    rows = batch // CELL_CHUNKS
    me = lax.axis_index("tp")
    place = lax.rem(me, group)
    first = me - place
    head = lax.div(me, group)
    barrier = pltpu.get_barrier_semaphore()
    for i in range(1, n):
        pl.semaphore_signal(
            barrier,
            inc=1,
            device_id={"tp": lax.rem(me + i, n)},
            device_id_type=pl.DeviceIdType.MESH,
        )

    def fetch(source, target, sem):
        copy = pltpu.make_async_copy(source, target, sem)
        copy.start()
        return copy

    small = [
        fetch(source, target, small_sem.at[i])
        for i, (source, target) in enumerate(
            [
                (tokens, tok_buf),
                (norm_gain, gain_buf),
                (w_gates, gate_buf),
                (bias_forget, bias_buf),
                (stab, stab_buf),
            ]
        )
    ]
    norm_copy = fetch(norm_vec, norm_buf.at[place], small_sem.at[5])
    names = [w_query, w_key, w_value, w_outgate, w_proj]
    weight_copies = [[None] * 5 for _ in range(layers)]
    cell_copies = [[None] * CELL_CHUNKS for _ in range(layers)]

    def fetch_weights(layer):
        for i in range(4):
            weight_copies[layer][i] = fetch(
                names[i].at[layer],
                weights.at[layer, pl.ds(i * ncols, ncols)],
                weight_sem.at[layer, i],
            )

    def fetch_cell(layer):
        for c in range(CELL_CHUNKS):
            part = pl.ds(c * rows, rows)
            cell_copies[layer][c] = fetch(
                cell.at[layer, part], cell_buf.at[layer, part], cell_sem.at[layer, c]
            )
        weight_copies[layer][4] = fetch(
            names[4].at[layer],
            weights.at[layer, pl.ds(4 * ncols, ncols)],
            weight_sem.at[layer, 4],
        )

    fetch_weights(0)

    def to_group(source, send, recv):
        copies = []
        for i in range(1, group):
            copy = pltpu.make_async_remote_copy(
                src_ref=source.at[place],
                dst_ref=source.at[place],
                send_sem=send.at[i],
                recv_sem=recv.at[i],
                device_id={"tp": first + lax.rem(place + i, group)},
                device_id_type=pl.DeviceIdType.MESH,
            )
            copy.start()
            copies.append(copy)
        return copies

    def finish_group(copies, source, recv):
        for i, copy in enumerate(copies, 1):
            origin = lax.rem(place + group - i, group)
            pltpu.make_async_copy(source.at[origin], source.at[origin], recv.at[i]).wait()
            copy.wait_send()

    chips = n // 2
    core = lax.rem(me, 2)
    chip = lax.div(me, 2)

    def push(buffer, at, target, send, recv):
        copy = pltpu.make_async_remote_copy(
            src_ref=buffer.at[at],
            dst_ref=buffer.at[at],
            send_sem=send,
            recv_sem=recv,
            device_id={"tp": target},
            device_id_type=pl.DeviceIdType.MESH,
        )
        copy.start()
        return copy

    def to_all(buffer, send, recv):
        copies = [
            push(buffer, me, lax.rem(chip + i, chips) * 2 + core, send.at[0, i], recv.at[0, i])
            for i in range(1, chips)
        ]
        copies.append(push(buffer, me, chip * 2 + 1 - core, send.at[1, 0], recv.at[1, 0]))
        return copies

    def finish_all(copies, buffer, send, recv):
        for i in range(1, chips):
            origin = lax.rem(chip + chips - i, chips) * 2 + core
            pltpu.make_async_copy(buffer.at[origin], buffer.at[origin], recv.at[0, i]).wait()
            copies.append(
                push(buffer, origin, chip * 2 + 1 - core, send.at[1, i], recv.at[1, i])
            )
        for i in range(chips):
            origin = lax.rem(chip + chips - i, chips) * 2 + 1 - core
            pltpu.make_async_copy(buffer.at[origin], buffer.at[origin], recv.at[1, i]).wait()
        for copy in copies:
            copy.wait_send()

    for copy in small:
        copy.wait()
    norm_copies = None
    own = tok_buf[:, pl.ds(pl.multiple_of(me * ncols, ncols), ncols)].astype(jnp.float32)
    for layer in range(layers):
        if layer == 0:
            current = tok_buf[...].astype(jnp.float32)
        else:
            current = jnp.concatenate(
                [result_buf[layer - 1, d] for d in range(n)], axis=1
            ).astype(jnp.float32)
        mean = jnp.sum(current * current, axis=-1, keepdims=True) * (1.0 / width)
        normed = (current * lax.rsqrt(mean + epsilon) * gain_buf[pl.ds(layer, 1), :]).astype(
            jnp.bfloat16
        )
        for i in range(4):
            weight_copies[layer][i].wait()
        if layer == 0:
            fetch_cell(layer)
        both = lax.dot_general(
            normed, weights[layer, : 2 * ncols], NT, preferred_element_type=jnp.float32
        )
        query = both[:, :ncols].astype(jnp.bfloat16)
        key = (both[:, ncols:] * dh ** (-0.5)).astype(jnp.bfloat16)
        pair_buf[layer, place, 0] = query
        pair_buf[layer, place, 1] = key
        if layer == 0:
            norm_copy.wait()
            pl.semaphore_wait(barrier, n - 1)
        pair_copies = to_group(pair_buf.at[layer], pair_send.at[layer], pair_recv.at[layer])
        if layer == 0:
            norm_copies = to_group(norm_buf, norm_send, norm_recv)
        both = lax.dot_general(
            normed,
            weights[layer, 2 * ncols : 4 * ncols],
            NT,
            preferred_element_type=jnp.float32,
        )
        value = both[:, :ncols].astype(jnp.bfloat16).astype(jnp.float32)
        outgate = both[:, ncols:].astype(jnp.bfloat16).astype(jnp.float32)
        gates = lax.dot_general(
            normed, gate_buf[layer], NT, preferred_element_type=jnp.float32
        )
        in_gate = gates[:, :heads]
        forget = gates[:, heads:] + bias_buf[pl.ds(layer, 1), :]
        log_forget = jnp.minimum(forget, 0.0) - jnp.log1p(jnp.exp(-jnp.abs(forget)))
        old_stab = stab_buf[layer].T
        next_stab = jnp.maximum(log_forget + old_stab, in_gate)
        new_stab[layer] = next_stab.T
        mine = lax.broadcasted_iota(jnp.int32, (batch, heads), 1) == head

        def pick(entry):
            return jnp.sum(jnp.where(mine, entry, 0.0), axis=-1, keepdims=True)

        my_stab = pick(next_stab)
        my_decay = jnp.exp(pick(log_forget + old_stab) - my_stab)
        my_weight = jnp.exp(pick(in_gate) - my_stab)
        new_norm[layer] = my_decay * norm_buf[place, layer] + my_weight * key.astype(jnp.float32)
        weighted = my_weight * value
        wv_buf[layer] = weighted
        decay_buf[layer] = jnp.broadcast_to(my_decay, (batch, ncols))
        gate = jax.nn.sigmoid(outgate)

        finish_group(pair_copies, pair_buf.at[layer], pair_recv.at[layer])
        if layer == 0:
            finish_group(norm_copies, norm_buf, norm_recv)
        q_head = jnp.concatenate([pair_buf[layer, j, 0] for j in range(group)], axis=1)
        q_head = q_head.astype(jnp.float32)
        k_head = jnp.concatenate([pair_buf[layer, j, 1] for j in range(group)], axis=1)
        k_head = k_head.astype(jnp.float32)
        n_head = jnp.concatenate([norm_buf[j, layer] for j in range(group)], axis=1)
        key_buf[layer] = k_head
        denom = jnp.sum(
            q_head * (my_decay * n_head + my_weight * k_head), axis=-1, keepdims=True
        )
        inner = jnp.sum(q_head * k_head, axis=-1, keepdims=True)

        def read_rows(c, start, layer=layer):
            queries = jnp.concatenate(
                [pair_buf[layer, j, 0, pl.ds(start, rows), :] for j in range(group)], axis=1
            )
            row = lax.broadcasted_iota(jnp.int32, (rows, ncols), 0)
            total = jnp.zeros((rows, ncols), jnp.float32)
            for b in range(rows):
                block = cell_buf[layer, start + b].astype(jnp.bfloat16)
                product = lax.dot_general(
                    queries, block, NT, preferred_element_type=jnp.float32
                )
                total = jnp.where(row == b, product, total)
            numer_buf[pl.ds(start, rows), :] = total

        for c in range(CELL_CHUNKS):
            cell_copies[layer][c].wait()
            read_rows(c, c * rows)
        numer = my_decay * numer_buf[...] + weighted * inner
        readout = numer / jnp.maximum(jnp.abs(denom), jnp.exp(-my_stab))
        branch_buf[layer, me] = (gate * readout).astype(jnp.bfloat16)
        branch_copies = to_all(
            branch_buf.at[layer], gather_send.at[layer, 0], gather_recv.at[layer, 0]
        )
        if layer + 1 < layers:
            fetch_weights(layer + 1)
            fetch_cell(layer + 1)

        weight_copies[layer][4].wait()
        finish_all(
            branch_copies,
            branch_buf.at[layer],
            gather_send.at[layer, 0],
            gather_recv.at[layer, 0],
        )
        branch = jnp.concatenate([branch_buf[layer, d] for d in range(n)], axis=1)
        summed = lax.dot_general(
            branch,
            weights[layer, 4 * ncols : 5 * ncols],
            NT,
            preferred_element_type=jnp.float32,
        )
        result = (own + summed).astype(jnp.bfloat16)
        own = result.astype(jnp.float32)
        if layer + 1 < layers:
            result_buf[layer, me] = result
            result_copies = to_all(
                result_buf.at[layer], gather_send.at[layer, 1], gather_recv.at[layer, 1]
            )
            finish_all(
                result_copies,
                result_buf.at[layer],
                gather_send.at[layer, 1],
                gather_recv.at[layer, 1],
            )
        else:
            mixed[...] = result


def fused_body(n, *args):
    (tokens, norm_gain, w_query, _, _, _, w_gates, bias_forget, _, cell, norm_vec, stab) = args
    layers, batch, ncols, dh = cell.shape
    width = tokens.shape[1]
    group = dh // ncols
    w_gates = jnp.swapaxes(w_gates, 1, 2)
    stab = jnp.swapaxes(stab, 1, 2)
    args = args[:6] + (w_gates,) + args[7:11] + (stab,)
    args = [pltpu.with_memory_space_constraint(arg, pltpu.HBM) for arg in args]
    bf16, f32 = jnp.bfloat16, jnp.float32
    vmem = pl.BlockSpec(memory_space=pltpu.VMEM)
    dma = pltpu.SemaphoreType.DMA
    mixed, held, new_norm, new_stab, weighted, keys, decay = pl.pallas_call(
        functools.partial(fused_kernel, n, group),
        out_shape=(
            jax.ShapeDtypeStruct((batch, ncols), bf16),
            pltpu.VMEM(cell.shape, f32),
            jax.ShapeDtypeStruct(norm_vec.shape, f32),
            jax.ShapeDtypeStruct(stab.shape, f32),
            jax.ShapeDtypeStruct((layers, batch, ncols), f32),
            jax.ShapeDtypeStruct((layers, batch, dh), f32),
            jax.ShapeDtypeStruct((layers, batch, ncols), f32),
        ),
        in_specs=[pl.BlockSpec(memory_space=pltpu.HBM)] * len(args),
        out_specs=(vmem,) * 7,
        scratch_shapes=[
            pltpu.VMEM(tokens.shape, bf16),
            pltpu.VMEM(norm_gain.shape, f32),
            pltpu.VMEM((layers, 5 * ncols, width), bf16),
            pltpu.VMEM(w_gates.shape, bf16),
            pltpu.VMEM(bias_forget.shape, f32),
            pltpu.VMEM(stab.shape, f32),
            pltpu.VMEM((group,) + norm_vec.shape, f32),
            pltpu.VMEM((layers, group, 2, batch, ncols), bf16),
            pltpu.VMEM((layers, n, batch, ncols), bf16),
            pltpu.VMEM((layers, n, batch, ncols), bf16),
            pltpu.VMEM((batch, ncols), f32),
            dma((6,)),
            dma((layers, 5)),
            dma((layers, CELL_CHUNKS)),
            dma((group,)),
            dma((group,)),
            dma((layers, group)),
            dma((layers, group)),
            dma((layers, 2, 2, n // 2)),
            dma((layers, 2, 2, n // 2)),
        ],
        compiler_params=pltpu.CompilerParams(
            collective_id=0, has_side_effects=True, vmem_limit_bytes=VMEM_LIMIT
        ),
        name="cells",
    )(*args)
    new_cell = (
        decay[:, :, :1, None] * held + weighted[:, :, :, None] * keys[:, :, None, :]
    )
    mixed, new_norm, new_stab = write_small(mixed, new_norm, new_stab)
    return mixed, new_cell, new_norm, jnp.swapaxes(new_stab, 1, 2)


def write_kernel(*refs):
    half = len(refs) // 2
    sems = refs[-1]
    copies = [
        pltpu.make_async_copy(refs[i], refs[half + i], sems.at[i]) for i in range(half)
    ]
    for copy in copies:
        copy.start()
    for copy in copies:
        copy.wait()


def write_small(*arrays):
    return pl.pallas_call(
        write_kernel,
        out_shape=[jax.ShapeDtypeStruct(x.shape, x.dtype) for x in arrays],
        in_specs=[pl.BlockSpec(memory_space=pltpu.VMEM)] * len(arrays),
        out_specs=[pl.BlockSpec(memory_space=pltpu.HBM)] * len(arrays),
        scratch_shapes=[pltpu.SemaphoreType.DMA((len(arrays),))],
        compiler_params=pltpu.CompilerParams(vmem_limit_bytes=2**20),
        name="write",
    )(*arrays)


VMEM_LIMIT = 24 * 2**20


def whole_body(*args):
    n = lax.axis_size("tp")
    _, batch, ncols, dh = args[9].shape
    if n % 2 == 0 and ncols % 128 == 0 and dh % ncols == 0 and batch % (16 * CELL_CHUNKS) == 0:
        return fused_body(n, *args)
    return body(*args)


def solution(mesh):
    return jax.shard_map(
        whole_body,
        mesh=mesh,
        in_specs=(
            P("grp", None),
            P(),
            P(None, "tp", None),
            P(None, "tp", None),
            P(None, "tp", None),
            P(None, "tp", None),
            P(),
            P(),
            P(None, "tp", None),
            P(None, "grp", "tp", None),
            P(None, "grp", "tp"),
            P(None, "grp", None),
        ),
        out_specs=(
            P("grp", "tp"),
            P(None, "grp", "tp", None),
            P(None, "grp", "tp"),
            P(None, "grp", None),
        ),
        check_vma=False,
    )
```

profile of v0, /device:TPU:0, one launch (start us, length us, event | category | flops | bytes accessed | tf_op | source)
XLA Modules:
  0.0 41.1 jit_solution(11256401918709460468)
XLA Ops:
  0.6 32.6 %cells.1 = (bf16[64,128]{1,0:T(8,128)(2,1)S(1)}, f32[2,64,128,256]{3,2,1,0:T(8,128)S(1)}, f32[2,64,128]{2,1,0:T(8,128)S(1)}, f32[2,8,64]{2,1,0:T(8,128)S(1)}, f3...) custom-call(bf16[64,2048]{1,0:T(8,128)(2,1)} %tokens.1, f32[2,2048]{1,0:T(2,128)} %norm_gain.1, ...), custom_call_target="tpu_custom_call" | custom-call | tf_op jit(solution)/shard_map/cells/pallas_call | solution.py:465
  33.2 0.7 %write.1 = (bf16[64,128]{1,0:T(8,128)(2,1)}, f32[2,64,128]{2,1,0:T(8,128)}, f32[2,8,64]{2,1,0:T(8,128)}) custom-call(bf16[64,128]{1,0:T(8,128)(2,1)S(1)} %get-tuple-element.14.refs_0_, f32[2,64,128]{2,1,0:T(8,128)S(1)} %get-tuple-element.15.refs_1_, f32[2,8,64]{2,1,0:T(8,128)S(1)} %get-tuple-element.16.refs_2_), custom_call_target="tpu_custom_call" | custom-call | tf_op jit(solution)/shard_map/write/pallas_call | solution.py:525
  33.9 0.1 slice_reduce_fusion
  34.0 7.1 %multiply_add_fusion = f32[2,64,128,256]{3,2,1,0:T(8,128)} fusion(f32[2,64,128,256]{3,2,1,0:T(8,128)S(1)} %get-tuple-element.19, f32[2,64,256]{2,1,0:T(8,128)S(1)} %get-tuple-element.21, f32[2,64,128]{2,1,0:T(8,128)S(1)} %get-tuple-element.20, f32[2,64]{1,0:T(2,128)S(1)} %slice_reduce_fusion), kind=kLoop, calls=%fused_computation | loop fusion | flops 12582912 | bytes 33751552 | tf_op jit(solution)/shard_map/add | solution.py:506
where the time goes:
time: 41.2 us; the launch traced here: 41.1 us
  Pallas kernels  33.3 us (81%)
  other arithmetic  7.07 us (17%)
  between operations  0.65 us (2%)
    pallas_call x1, Pallas kernels, fused_body(): pl.pallas_call(functools.partial(fused_kernel, n, group), out_shape=(jax....  32.6 us
    add x1, other arithmetic, fused_body(): decay[:, :, :1, None] * held + weighted[:, :, :, None] * keys[:, :, None, :]  7.07 us

commit v1 on v0

v1 whole, which is shorter than its diff:
```python
import functools

import jax
import jax.numpy as jnp
from jax import lax
from jax.experimental import pallas as pl
from jax.experimental.pallas import tpu as pltpu
from jax.sharding import PartitionSpec as P

D = 2048
DH = 256
LAYERS = 2


epsilon = 1e-06


def from_partner(value, axis, apart):
    mask = 2**apart
    pairs = [(source, source ^ mask) for source in range(lax.axis_size(axis))]
    return lax.ppermute(value, axis, pairs)


def project(normed, weight):
    return lax.dot_general(
        normed, weight, (((1,), (1,)), ((), ())), preferred_element_type=jnp.float32
    )


def split_pieces(value):
    high = lax.optimization_barrier(value.astype(jnp.bfloat16))
    rest = value - high.astype(jnp.float32)
    middle = lax.optimization_barrier(rest.astype(jnp.bfloat16))
    lowest = (rest - middle.astype(jnp.float32)).astype(jnp.bfloat16)
    return jnp.stack([high, middle, lowest], axis=1)


def join_pieces(pieces):
    return jnp.sum(pieces.astype(jnp.float32), axis=-1)


def combine_halves(mine, theirs, lower):
    return jnp.where(
        lower, jnp.concatenate([mine, theirs], axis=1), jnp.concatenate([theirs, mine], axis=1)
    )


def one_cell(
    current,
    gain,
    w_query,
    w_key,
    w_value,
    w_outgate,
    w_gates,
    bias_forget,
    w_proj,
    cell,
    norm_vec,
    stab,
):
    heads = D // DH
    ncols = w_query.shape[0]
    group = DH // ncols
    device = lax.axis_index("tp")
    head = device // group
    cur_f = current.astype(jnp.float32)
    normed = (
        cur_f * lax.rsqrt(jnp.mean(cur_f * cur_f, axis=-1, keepdims=True) + epsilon) * gain
    ).astype(jnp.bfloat16)
    query = project(normed, w_query).astype(jnp.bfloat16)
    keys = (project(normed, w_key) * DH ** (-0.5)).astype(jnp.bfloat16)
    values = project(normed, w_value).astype(jnp.bfloat16)
    outgate = project(normed, w_outgate).astype(jnp.bfloat16)
    gates = jnp.dot(normed, w_gates, preferred_element_type=jnp.float32)
    in_gate = gates[:, :heads]
    log_forget = jax.nn.log_sigmoid(gates[:, heads:] + bias_forget)
    new_stab = jnp.maximum(log_forget + stab, in_gate)
    decay = jnp.exp(log_forget + stab - new_stab)
    weight_in = jnp.exp(in_gate - new_stab)
    select = (jnp.arange(heads) == head).astype(jnp.float32)
    my_decay = jnp.sum(decay * select, axis=-1)
    my_weight = jnp.sum(weight_in * select, axis=-1)
    my_stab = jnp.sum(new_stab * select, axis=-1)
    new_norm = my_decay[:, None] * norm_vec + my_weight[:, None] * keys.astype(jnp.float32)
    den_part = jnp.sum(query.astype(jnp.float32) * new_norm, axis=-1)
    q_head, k_head = (query, keys)
    denom = den_part
    for bit in range(group.bit_length() - 1):
        other_q, other_k, other_pieces = from_partner(
            (q_head, k_head, split_pieces(denom)), "tp", bit
        )
        lower = device // 2**bit % 2 == 0
        q_head = combine_halves(q_head, other_q, lower)
        k_head = combine_halves(k_head, other_k, lower)
        denom = denom + join_pieces(other_pieces)
    outer = values.astype(jnp.float32)[:, :, None] * k_head.astype(jnp.float32)[:, None, :]
    new_cell = my_decay[:, None, None] * cell + my_weight[:, None, None] * outer
    numer = jnp.einsum(
        "bk,bek->be", q_head.astype(jnp.float32), new_cell, precision=lax.Precision.HIGHEST
    )
    readout = numer / jnp.maximum(jnp.abs(denom), jnp.exp(-my_stab))[:, None]
    branch = (jax.nn.sigmoid(outgate.astype(jnp.float32)) * readout).astype(jnp.bfloat16)
    summed = project(lax.all_gather(branch, "tp", axis=1, tiled=True), w_proj)
    own_input = lax.dynamic_slice_in_dim(cur_f, device * ncols, ncols, 1)
    result = (own_input + summed).astype(jnp.bfloat16)
    return (result, new_cell, new_norm, new_stab)


def body(
    tokens,
    norm_gain,
    query_weight,
    key_weight,
    value_weight,
    outgate_weight,
    gate_weight,
    forget_bias,
    proj_weight,
    cell_state,
    normalizer,
    stabilizer,
):
    current = tokens
    cells = []
    norms = []
    stabs = []
    result = tokens
    for layer in range(LAYERS):
        result, new_cell, new_norm, new_stab = one_cell(
            current,
            norm_gain[layer],
            query_weight[layer],
            key_weight[layer],
            value_weight[layer],
            outgate_weight[layer],
            gate_weight[layer],
            forget_bias[layer],
            proj_weight[layer],
            cell_state[layer],
            normalizer[layer],
            stabilizer[layer],
        )
        cells.append(new_cell)
        norms.append(new_norm)
        stabs.append(new_stab)
        if layer + 1 < LAYERS:
            current = lax.all_gather(result, "tp", axis=1, tiled=True)
    return (result, jnp.stack(cells), jnp.stack(norms), jnp.stack(stabs))


NT = (((1,), (1,)), ((), ()))
CELL_CHUNKS = 4
MAIN_VMEM = 24 * 2**20
LAST_VMEM = 6 * 2**20


def flip(index, mask):
    result = index
    bit = 1
    while bit <= mask:
        if mask & bit:
            result = result + bit - 2 * bit * lax.rem(lax.div(index, bit), 2)
        bit *= 2
    return result


def fetch(source, target, sem):
    copy = pltpu.make_async_copy(source, target, sem)
    copy.start()
    return copy


def push(source, dest, target, send, recv):
    copy = pltpu.make_async_remote_copy(
        src_ref=source,
        dst_ref=dest,
        send_sem=send,
        recv_sem=recv,
        device_id={"tp": target},
        device_id_type=pl.DeviceIdType.MESH,
    )
    copy.start()
    return copy


def arrived(buffer, recv):
    pltpu.make_async_copy(buffer, buffer, recv).wait()


def greet_all(n, me):
    barrier = pltpu.get_barrier_semaphore()
    for i in range(1, n):
        pl.semaphore_signal(
            barrier,
            inc=1,
            device_id={"tp": lax.rem(me + i, n)},
            device_id_type=pl.DeviceIdType.MESH,
        )
    return barrier


def read_rows(cell_rows, queries, numer, start, rows):
    ncols = numer.shape[1]
    row = lax.broadcasted_iota(jnp.int32, (rows, ncols), 0)
    total = jnp.zeros((rows, ncols), jnp.float32)
    for b in range(rows):
        block = cell_rows(start + b).astype(jnp.bfloat16)
        product = lax.dot_general(queries, block, NT, preferred_element_type=jnp.float32)
        total = jnp.where(row == b, product, total)
    numer[pl.ds(start, rows), :] = total


def send_half(half, chip, core, chips, rows, source, dest, send, recv):
    me = chip * 2 + core
    return [
        push(
            source.at[pl.ds(half * rows, rows)],
            dest.at[me],
            flip(chip, m) * 2 + half,
            send.at[half, m],
            recv.at[m, core],
        )
        for m in range(chips - 1, 0, -1)
    ]


def gather_project(chip, core, chips, rows, source, dest, send, recv, weights, copies):
    me = chip * 2 + core
    partner = chip * 2 + 1 - core
    ncols = dest.shape[2]
    copies.append(
        push(
            source.at[pl.ds(pl.multiple_of((1 - core) * rows, rows), rows)],
            dest.at[me],
            partner,
            send.at[0, 0],
            recv.at[0, core],
        )
    )
    dest[me] = source[pl.ds(pl.multiple_of(core * rows, rows), rows), :]
    total = jnp.zeros((rows, 2 * ncols), jnp.float32)
    for m in range(chips):
        other = flip(chip, m)
        if m == 0:
            arrived(dest.at[partner], recv.at[0, 1 - core])
        else:
            for c in range(2):
                arrived(dest.at[other * 2 + c], recv.at[m, c])
        block = jnp.concatenate([dest[other * 2], dest[other * 2 + 1]], axis=1)
        part = weights[:, pl.ds(pl.multiple_of(other * 2 * ncols, 2 * ncols), 2 * ncols)]
        total = total + lax.dot_general(block, part, NT, preferred_element_type=jnp.float32)
    return total


def cells_kernel(
    n,
    tokens,
    norm_gain,
    w_query,
    w_key,
    w_value,
    w_outgate,
    w_gates,
    bias_forget,
    w_proj,
    cell,
    norm_vec,
    stab,
    cell_buf,
    new_norm,
    new_stab,
    wv_buf,
    key_buf,
    decay_buf,
    q_out,
    inner_out,
    den_out,
    gate_out,
    own_out,
    tok_buf,
    gain_buf,
    weights,
    wide,
    proj_buf,
    gate_buf,
    bias_buf,
    stab_buf,
    norm_buf,
    pair_buf,
    send_buf,
    branch_buf,
    result_buf,
    whole_buf,
    swap_buf,
    swap_out,
    gates_buf,
    numer_buf,
    small_sem,
    weight_sem,
    wide_sem,
    cell_sem,
    pair_send,
    pair_recv,
    branch_send,
    branch_recv,
    result_send,
    result_recv,
):
    layers, batch, ncols, dh = cell.shape
    width = tokens.shape[1]
    heads = stab.shape[1]
    rows = batch // CELL_CHUNKS
    half = batch // 2
    chips = n // 2
    me = lax.axis_index("tp")
    core = lax.rem(me, 2)
    chip = lax.div(me, 2)
    partner = chip * 2 + 1 - core
    barrier = greet_all(n, me)

    tok_copy = fetch(tokens, tok_buf, small_sem.at[0])
    gain_copy = fetch(norm_gain, gain_buf, small_sem.at[1])
    names = [w_query, w_key, w_value, w_outgate]
    weight_copies = [
        fetch(names[i].at[0], weights.at[pl.ds(i * ncols, ncols)], weight_sem.at[i])
        for i in range(4)
    ]
    small = [
        fetch(w_gates, gate_buf, small_sem.at[2]),
        fetch(bias_forget, bias_buf, small_sem.at[3]),
        fetch(stab, stab_buf, small_sem.at[4]),
    ]
    norm_copy = fetch(norm_vec, norm_buf.at[core], small_sem.at[5])

    def fetch_cell(layer):
        return [
            fetch(
                cell.at[layer, pl.ds(c * rows, rows)],
                cell_buf.at[layer, pl.ds(c * rows, rows)],
                cell_sem.at[layer, c],
            )
            for c in range(CELL_CHUNKS)
        ]

    def own_rows(ref, i):
        return ref.at[pl.ds(pl.multiple_of(i * 2 * ncols + core * ncols, ncols), ncols)]

    def scale(gates, layer):
        in_gate = gates[:, :heads]
        forget = gates[:, heads : 2 * heads] + bias_buf[pl.ds(layer, 1), :]
        log_forget = jnp.minimum(forget, 0.0) - jnp.log1p(jnp.exp(-jnp.abs(forget)))
        old_stab = stab_buf[layer].T
        next_stab = jnp.maximum(log_forget + old_stab, in_gate)
        new_stab[layer] = next_stab.T
        mine = lax.broadcasted_iota(jnp.int32, (batch, heads), 1) == chip

        def pick(entry):
            return jnp.sum(jnp.where(mine, entry, 0.0), axis=-1, keepdims=True)

        my_stab = pick(next_stab)
        my_decay = jnp.exp(pick(log_forget + old_stab) - my_stab)
        my_weight = jnp.exp(pick(in_gate) - my_stab)
        return my_stab, my_decay, my_weight

    def finish_head(layer, q_head, k_head, my_stab, my_decay, my_weight):
        n_head = jnp.concatenate([norm_buf[j, layer] for j in range(2)], axis=1)
        denom = jnp.sum(
            q_head * (my_decay * n_head + my_weight * k_head), axis=-1, keepdims=True
        )
        inner = jnp.sum(q_head * k_head, axis=-1, keepdims=True)
        return inner, jnp.maximum(jnp.abs(denom), jnp.exp(-my_stab))

    tok_copy.wait()
    gain_copy.wait()
    current = tok_buf[...].astype(jnp.float32)
    mean = jnp.sum(current * current, axis=-1, keepdims=True) * (1.0 / width)
    normed = (current * lax.rsqrt(mean + epsilon) * gain_buf[0:1, :]).astype(jnp.bfloat16)
    weight_copies[0].wait()
    weight_copies[1].wait()
    both = lax.dot_general(
        normed, weights[: 2 * ncols], NT, preferred_element_type=jnp.float32
    )
    pair_buf[core, 0] = both[:, :ncols].astype(jnp.bfloat16)
    key = (both[:, ncols:] * dh ** (-0.5)).astype(jnp.bfloat16)
    pair_buf[core, 1] = key
    weight_copies[2].wait()
    weight_copies[3].wait()
    for copy in small:
        copy.wait()
    norm_copy.wait()
    proj_copy = fetch(w_proj.at[0], own_rows(proj_buf, 0), small_sem.at[6])
    cell_copies = fetch_cell(0)
    pl.semaphore_wait(barrier, n - 1)
    pair_copies = [
        push(pair_buf.at[core], pair_buf.at[core], partner, pair_send.at[0], pair_recv.at[0]),
        push(norm_buf.at[core], norm_buf.at[core], partner, pair_send.at[1], pair_recv.at[1]),
    ]
    both = lax.dot_general(
        normed, weights[2 * ncols :], NT, preferred_element_type=jnp.float32
    )
    value = both[:, :ncols].astype(jnp.bfloat16).astype(jnp.float32)
    gate = jax.nn.sigmoid(both[:, ncols:].astype(jnp.bfloat16).astype(jnp.float32))
    gates = lax.dot_general(normed, gate_buf[0], NT, preferred_element_type=jnp.float32)
    my_stab, my_decay, my_weight = scale(gates, 0)
    new_norm[0] = my_decay * norm_buf[core, 0] + my_weight * key.astype(jnp.float32)
    weighted = my_weight * value
    wv_buf[0] = weighted
    decay_buf[0] = jnp.broadcast_to(my_decay, (batch, ncols))
    arrived(pair_buf.at[1 - core], pair_recv.at[0])
    arrived(norm_buf.at[1 - core], pair_recv.at[1])
    proj_copy.wait()
    pair_copies.append(
        push(own_rows(proj_buf, 0), own_rows(proj_buf, 0), partner, pair_send.at[2], pair_recv.at[2])
    )
    q_head = jnp.concatenate([pair_buf[j, 0] for j in range(2)], axis=1).astype(jnp.float32)
    k_head = jnp.concatenate([pair_buf[j, 1] for j in range(2)], axis=1).astype(jnp.float32)
    key_buf[0] = k_head
    inner, den = finish_head(0, q_head, k_head, my_stab, my_decay, my_weight)

    branch_copies = []
    for h in range(2):
        for c in range(h * CELL_CHUNKS // 2, (h + 1) * CELL_CHUNKS // 2):
            cell_copies[c].wait()
            queries = jnp.concatenate(
                [pair_buf[j, 0, pl.ds(c * rows, rows), :] for j in range(2)], axis=1
            )
            read_rows(lambda b: cell_buf[0, b], queries, numer_buf, c * rows, rows)
        part = slice(h * half, (h + 1) * half)
        numer = my_decay[part] * numer_buf[part, :] + weighted[part] * inner[part]
        send_buf[part, :] = (gate[part] * (numer / den[part])).astype(jnp.bfloat16)
        branch_copies += send_half(
            h, chip, core, chips, half, send_buf, branch_buf, branch_send, branch_recv
        )
    wide_copies = [
        fetch(names[i].at[1], own_rows(wide, i), wide_sem.at[i]) for i in range(4)
    ]
    cell_copies = fetch_cell(1)
    arrived(
        proj_buf.at[pl.ds(pl.multiple_of((1 - core) * ncols, ncols), ncols)], pair_recv.at[2]
    )
    wide_pushes = []
    for i in range(4):
        wide_copies[i].wait()
        wide_pushes.append(
            push(
                own_rows(wide, i),
                own_rows(wide, i),
                partner,
                pair_send.at[3 + i],
                pair_recv.at[3 + i],
            )
        )
    summed = gather_project(
        chip,
        core,
        chips,
        half,
        send_buf,
        branch_buf,
        branch_send,
        branch_recv,
        proj_buf,
        branch_copies,
    )
    my_rows = pl.ds(pl.multiple_of(core * half, half), half)
    my_cols = pl.ds(pl.multiple_of(chip * 2 * ncols, 2 * ncols), 2 * ncols)
    result = (tok_buf[my_rows, my_cols].astype(jnp.float32) + summed).astype(jnp.bfloat16)
    own_out[...] = result
    result_buf[chip] = result
    result_copies = [
        push(
            result_buf.at[chip],
            result_buf.at[chip],
            flip(chip, m) * 2 + core,
            result_send.at[m],
            result_recv.at[m],
        )
        for m in range(chips - 1, 0, -1)
    ]

    for i in range(4):
        arrived(
            wide.at[pl.ds(pl.multiple_of(i * 2 * ncols + (1 - core) * ncols, ncols), ncols)],
            pair_recv.at[3 + i],
        )
    total = jnp.zeros((half, 8 * ncols), jnp.float32)
    gates = jnp.zeros((half, 2 * heads), jnp.float32)
    square = jnp.zeros((half, 1), jnp.float32)
    for m in range(chips):
        other = flip(chip, m)
        if m:
            arrived(result_buf.at[other], result_recv.at[m])
        cols = pl.ds(pl.multiple_of(other * 2 * ncols, 2 * ncols), 2 * ncols)
        block = result_buf[other].astype(jnp.float32)
        square = square + jnp.sum(block * block, axis=-1, keepdims=True)
        block = (block * gain_buf[1:2, cols]).astype(jnp.bfloat16)
        total = total + lax.dot_general(
            block, wide[:, cols], NT, preferred_element_type=jnp.float32
        )
        gates = gates + lax.dot_general(
            block, gate_buf[1, :, cols], NT, preferred_element_type=jnp.float32
        )
    root = lax.rsqrt(square * (1.0 / width) + epsilon)
    total = total * root
    query = total[:, : 2 * ncols].astype(jnp.bfloat16)
    key = (total[:, 2 * ncols : 4 * ncols] * dh ** (-0.5)).astype(jnp.bfloat16)
    whole_buf[...] = total[:, 4 * ncols :].astype(jnp.bfloat16)
    for target, side in ((swap_buf.at[core], core), (swap_out, 1 - core)):
        target[:, : 2 * ncols] = query
        target[:, 2 * ncols : 4 * ncols] = key
        for i in range(2):
            target[:, (4 + i) * ncols : (5 + i) * ncols] = whole_buf[
                :, pl.ds(pl.multiple_of(i * 2 * ncols + side * ncols, ncols), ncols)
            ]
    gates_buf[core] = jnp.concatenate(
        [gates * root, jnp.zeros((half, ncols - 2 * heads), jnp.float32)], axis=1
    )
    pair_copies += [
        push(swap_out, swap_buf.at[core], partner, pair_send.at[7], pair_recv.at[7]),
        push(gates_buf.at[core], gates_buf.at[core], partner, pair_send.at[8], pair_recv.at[8]),
    ]
    for copy in branch_copies + wide_pushes + result_copies:
        copy.wait_send()
    for copy in cell_copies:
        copy.wait()
    arrived(swap_buf.at[1 - core], pair_recv.at[7])
    arrived(gates_buf.at[1 - core], pair_recv.at[8])

    def both_halves(part):
        return jnp.concatenate([swap_buf[j, :, part] for j in range(2)], axis=0)

    gates = jnp.concatenate([gates_buf[j] for j in range(2)], axis=0)
    my_stab, my_decay, my_weight = scale(gates, 1)
    queries = both_halves(slice(0, 2 * ncols))
    q_out[...] = queries
    q_head = queries.astype(jnp.float32)
    k_head = both_halves(slice(2 * ncols, 4 * ncols)).astype(jnp.float32)
    key_buf[1] = k_head
    key = both_halves(pl.ds(pl.multiple_of((2 + core) * ncols, ncols), ncols))
    new_norm[1] = my_decay * norm_buf[core, 1] + my_weight * key.astype(jnp.float32)
    weighted = my_weight * both_halves(slice(4 * ncols, 5 * ncols)).astype(jnp.float32)
    wv_buf[1] = weighted
    decay_buf[1] = jnp.broadcast_to(my_decay, (batch, ncols))
    gate_out[...] = jax.nn.sigmoid(both_halves(slice(5 * ncols, 6 * ncols)).astype(jnp.float32))
    inner, den = finish_head(1, q_head, k_head, my_stab, my_decay, my_weight)
    inner_out[...] = weighted * inner
    den_out[...] = jnp.broadcast_to(den, (batch, ncols))
    for copy in pair_copies:
        copy.wait_send()


def last_kernel(
    n,
    cell_buf,
    queries,
    decay,
    inner,
    den,
    gate,
    own,
    _,
    w_proj,
    mixed,
    proj_buf,
    send_buf,
    branch_buf,
    swap_buf,
    swap_out,
    numer_buf,
    proj_sem,
    pair_send,
    pair_recv,
    branch_send,
    branch_recv,
):
    layers, batch, ncols, dh = cell_buf.shape
    last = layers - 1
    rows = batch // CELL_CHUNKS
    half = batch // 2
    chips = n // 2
    me = lax.axis_index("tp")
    core = lax.rem(me, 2)
    chip = lax.div(me, 2)
    partner = chip * 2 + 1 - core
    barrier = greet_all(n, me)
    own_part = proj_buf.at[pl.ds(pl.multiple_of(core * ncols, ncols), ncols)]
    proj_copy = fetch(w_proj.at[last], own_part, proj_sem)
    copies = []
    for h in range(2):
        for c in range(h * CELL_CHUNKS // 2, (h + 1) * CELL_CHUNKS // 2):
            read_rows(
                lambda b: cell_buf[last, b],
                queries[pl.ds(c * rows, rows), :],
                numer_buf,
                c * rows,
                rows,
            )
        part = slice(h * half, (h + 1) * half)
        numer = decay[last, part, :] * numer_buf[part, :] + inner[part, :]
        send_buf[part, :] = (gate[part, :] * (numer / den[part, :])).astype(jnp.bfloat16)
        if h == 0:
            pl.semaphore_wait(barrier, n - 1)
        copies += send_half(
            h, chip, core, chips, half, send_buf, branch_buf, branch_send, branch_recv
        )
    proj_copy.wait()
    pair_copies = [push(own_part, own_part, partner, pair_send.at[0], pair_recv.at[0])]
    arrived(
        proj_buf.at[pl.ds(pl.multiple_of((1 - core) * ncols, ncols), ncols)], pair_recv.at[0]
    )
    summed = gather_project(
        chip,
        core,
        chips,
        half,
        send_buf,
        branch_buf,
        branch_send,
        branch_recv,
        proj_buf,
        copies,
    )
    result = (own[...].astype(jnp.float32) + summed).astype(jnp.bfloat16)
    swap_buf[...] = result
    swap_out[core] = swap_buf[:, pl.ds(pl.multiple_of((1 - core) * ncols, ncols), ncols)]
    pair_copies.append(
        push(swap_out.at[core], swap_out.at[2 + core], partner, pair_send.at[1], pair_recv.at[1])
    )
    mixed[pl.ds(pl.multiple_of(core * half, half), half), :] = swap_buf[
        :, pl.ds(pl.multiple_of(core * ncols, ncols), ncols)
    ]
    for copy in copies:
        copy.wait_send()
    arrived(swap_out.at[3 - core], pair_recv.at[1])
    mixed[pl.ds(pl.multiple_of((1 - core) * half, half), half), :] = swap_out[3 - core]
    for copy in pair_copies:
        copy.wait_send()


def fused_body(n, *args):
    (tokens, norm_gain, w_query, _, _, _, w_gates, bias_forget, _, cell, norm_vec, stab) = args
    layers, batch, ncols, dh = cell.shape
    width = tokens.shape[1]
    half = batch // 2
    chips = n // 2
    w_gates = jnp.swapaxes(w_gates, 1, 2)
    stab = jnp.swapaxes(stab, 1, 2)
    args = args[:6] + (w_gates,) + args[7:11] + (stab,)
    args = [pltpu.with_memory_space_constraint(arg, pltpu.HBM) for arg in args]
    bf16, f32 = jnp.bfloat16, jnp.float32
    vmem = pl.BlockSpec(memory_space=pltpu.VMEM)
    hbm = pl.BlockSpec(memory_space=pltpu.HBM)
    dma = pltpu.SemaphoreType.DMA
    rows = jax.ShapeDtypeStruct((batch, ncols), f32)
    held, new_norm, new_stab, weighted, keys, decay, queries, inner, den, gate, own = pl.pallas_call(
        functools.partial(cells_kernel, n),
        out_shape=(
            pltpu.VMEM(cell.shape, f32),
            jax.ShapeDtypeStruct(norm_vec.shape, f32),
            jax.ShapeDtypeStruct(stab.shape, f32),
            jax.ShapeDtypeStruct((layers, batch, ncols), f32),
            jax.ShapeDtypeStruct((layers, batch, dh), f32),
            jax.ShapeDtypeStruct((layers, batch, ncols), f32),
            jax.ShapeDtypeStruct((batch, dh), bf16),
            rows,
            rows,
            rows,
            jax.ShapeDtypeStruct((half, dh), bf16),
        ),
        in_specs=[hbm] * len(args),
        out_specs=(vmem,) * 11,
        scratch_shapes=[
            pltpu.VMEM(tokens.shape, bf16),
            pltpu.VMEM(norm_gain.shape, f32),
            pltpu.VMEM((4 * ncols, width), bf16),
            pltpu.VMEM((8 * ncols, width), bf16),
            pltpu.VMEM((2 * ncols, width), bf16),
            pltpu.VMEM(w_gates.shape, bf16),
            pltpu.VMEM(bias_forget.shape, f32),
            pltpu.VMEM(stab.shape, f32),
            pltpu.VMEM((2,) + norm_vec.shape, f32),
            pltpu.VMEM((2, 2, batch, ncols), bf16),
            pltpu.VMEM((batch, ncols), bf16),
            pltpu.VMEM((n, half, ncols), bf16),
            pltpu.VMEM((chips, half, 2 * ncols), bf16),
            pltpu.VMEM((half, 4 * ncols), bf16),
            pltpu.VMEM((2, half, 6 * ncols), bf16),
            pltpu.VMEM((half, 6 * ncols), bf16),
            pltpu.VMEM((2, half, ncols), f32),
            pltpu.VMEM((batch, ncols), f32),
            dma((7,)),
            dma((4,)),
            dma((4,)),
            dma((layers, CELL_CHUNKS)),
            dma((9,)),
            dma((9,)),
            dma((2, chips)),
            dma((chips, 2)),
            dma((chips,)),
            dma((chips,)),
        ],
        compiler_params=pltpu.CompilerParams(
            collective_id=0, has_side_effects=True, vmem_limit_bytes=MAIN_VMEM
        ),
        name="cells",
    )(*args)
    new_cell = (
        decay[:, :, :1, None] * held + weighted[:, :, :, None] * keys[:, :, None, :]
    )
    mixed = pl.pallas_call(
        functools.partial(last_kernel, n),
        out_shape=jax.ShapeDtypeStruct((batch, ncols), bf16),
        in_specs=[vmem] * 8 + [hbm],
        out_specs=vmem,
        scratch_shapes=[
            pltpu.VMEM((2 * ncols, width), bf16),
            pltpu.VMEM((batch, ncols), bf16),
            pltpu.VMEM((n, half, ncols), bf16),
            pltpu.VMEM((half, 2 * ncols), bf16),
            pltpu.VMEM((4, half, ncols), bf16),
            pltpu.VMEM((batch, ncols), f32),
            dma,
            dma((2,)),
            dma((2,)),
            dma((2, chips)),
            dma((chips, 2)),
        ],
        compiler_params=pltpu.CompilerParams(
            collective_id=1, has_side_effects=True, vmem_limit_bytes=LAST_VMEM
        ),
        cost_estimate=pl.CostEstimate(
            flops=5 * 10**10, bytes_accessed=10**6, transcendentals=0
        ),
        name="last",
    )(held, queries, decay, inner, den, gate, own, new_cell[0, 0, :8, :128], args[8])
    mixed, new_norm, new_stab = write_small(mixed, new_norm, new_stab)
    return mixed, new_cell, new_norm, jnp.swapaxes(new_stab, 1, 2)


def write_kernel(*refs):
    half = len(refs) // 2
    sems = refs[-1]
    copies = [
        pltpu.make_async_copy(refs[i], refs[half + i], sems.at[i]) for i in range(half)
    ]
    for copy in copies:
        copy.start()
    for copy in copies:
        copy.wait()


def write_small(*arrays):
    return pl.pallas_call(
        write_kernel,
        out_shape=[jax.ShapeDtypeStruct(x.shape, x.dtype) for x in arrays],
        in_specs=[pl.BlockSpec(memory_space=pltpu.VMEM)] * len(arrays),
        out_specs=[pl.BlockSpec(memory_space=pltpu.HBM)] * len(arrays),
        scratch_shapes=[pltpu.SemaphoreType.DMA((len(arrays),))],
        compiler_params=pltpu.CompilerParams(vmem_limit_bytes=2**20),
        name="write",
    )(*arrays)


def whole_body(*args):
    n = lax.axis_size("tp")
    layers, batch, ncols, dh = args[9].shape
    heads = args[11].shape[2]
    if (
        layers == 2
        and n == 2 * heads
        and n & (n - 1) == 0
        and ncols % 128 == 0
        and dh == 2 * ncols
        and batch % (16 * CELL_CHUNKS) == 0
    ):
        return fused_body(n, *args)
    return body(*args)


def solution(mesh):
    return jax.shard_map(
        whole_body,
        mesh=mesh,
        in_specs=(
            P("grp", None),
            P(),
            P(None, "tp", None),
            P(None, "tp", None),
            P(None, "tp", None),
            P(None, "tp", None),
            P(),
            P(),
            P(None, "tp", None),
            P(None, "grp", "tp", None),
            P(None, "grp", "tp"),
            P(None, "grp", None),
        ),
        out_specs=(
            P("grp", "tp"),
            P(None, "grp", "tp", None),
            P(None, "grp", "tp"),
            P(None, "grp", None),
        ),
        check_vma=False,
    )
```

time: 41.2 us -> 37.7 us (0.915)
  other arithmetic: 7.07 us -> 3.03 us
    add x1, other arithmetic: 7.07 us -> 3.03 us  [fused_body(): decay[:, :, :1, None] * held + weighted[:, :, :, None] * keys[:, :, None, :]]
    pallas_call x1 -> x2, Pallas kernels: 32.6 us -> 33.1 us  [the longest x1 23.9 us: fused_body(): pl.pallas_call(functools.partial(cells_kernel, n), out_shape=(pltpu.VMEM(...]
where the time goes in v1:
time: 37.7 us; the launch traced here: 37.6 us
  Pallas kernels  33.7 us (89%)
  other arithmetic  3.03 us (8%)
  between operations  0.68 us (2%)
    pallas_call x1, Pallas kernels, fused_body(): pl.pallas_call(functools.partial(cells_kernel, n), out_shape=(pltpu.VMEM(...  23.9 us
    pallas_call x1, Pallas kernels, fused_body(): pl.pallas_call(functools.partial(last_kernel, n), out_shape=jax.ShapeDtyp...  9.22 us
    add x1, other arithmetic, fused_body(): decay[:, :, :1, None] * held + weighted[:, :, :, None] * keys[:, :, None, :]  3.03 us

profile of v1, /device:TPU:0, one launch (start us, length us, event | category | flops | bytes accessed | tf_op | source)
XLA Modules:
  0.0 37.6 jit_solution(17195679700658013077)
XLA Ops:
  0.6 23.9 %cells.1 = (f32[2,64,128,256]{3,2,1,0:T(8,128)S(1)}, f32[2,64,128]{2,1,0:T(8,128)S(1)}, f32[2,8,64]{2,1,0:T(8,128)S(1)}, f32[2,64,128]{2,1,0:T(8,128)S(1)}, f32[...) custom-call(bf16[64,2048]{1,0:T(8,128)(2,1)} %tokens.1, ...), custom_call_target="tpu_custom_call" | custom-call | tf_op jit(solution)/shard_map/cells/pallas_call | solution.py:656
  24.5 0.1 slice_reduce_fusion
  24.6 3.0 %multiply_add_fusion = f32[2,64,128,256]{3,2,1,0:T(8,128)S(1)} fusion(f32[2,64,128,256]{3,2,1,0:T(8,128)S(1)} %get-tuple-element.18.cell_buf, f32[2,64,256]{2,1,0:T(8,128)S(1)} %get-tuple-element.26, f32[2,64,128]{2,1,0:T(8,128)S(1)} %get-tuple-element.25, f32[2,64]{1,0:T(2,128)S(1)} %slice_reduce_fusion), kind=kLoop, calls=%fused_computation | loop fusion | flops 12582912 | bytes 33751552 | tf_op jit(solution)/shard_map/add | solution.py:709
  27.6 0.0 copy-start
  27.7 9.2 %last.1.refs_0_ = bf16[64,128]{1,0:T(8,128)(2,1)S(1)} custom-call(f32[2,64,128,256]{3,2,1,0:T(8,128)S(1)} %get-tuple-element.18.cell_buf, bf16[64,256]{1,0:T(8,128)(2,1)S(1)} %get-tuple-element.19.queries, f32[2,64,128]{2,1,0:T(8,128)S(1)} %get-tuple-element.20.decay, f32[64,128]{1,0:T(8,128)S(1)} %get-tuple-element.21.inner, ...), custom_call_target="tpu_custom_call" | custom-call | flops 49999998976 | bytes 1000000 | tf_op jit(solution)/shard_map/last/pallas_call | solution.py:711
  36.9 0.0 copy-done
  36.9 0.7 %write.1 = (bf16[64,128]{1,0:T(8,128)(2,1)}, f32[2,64,128]{2,1,0:T(8,128)}, f32[2,8,64]{2,1,0:T(8,128)}) custom-call(bf16[64,128]{1,0:T(8,128)(2,1)S(1)} %last.1.refs_0_, f32[2,64,128]{2,1,0:T(8,128)S(1)} %get-tuple-element.27.refs_1_, f32[2,8,64]{2,1,0:T(8,128)S(1)} %get-tuple-element.28.refs_2_), custom_call_target="tpu_custom_call" | custom-call | tf_op jit(solution)/shard_map/write/pallas_call | solution.py:754
  (1 shorter events, 0.0 us)
Async XLA Ops:
  27.6 9.3 %copy-start = (f32[2,64,128,256]{3,2,1,0:T(8,128)}, f32[2,64,128,256]{3,2,1,0:T(8,128)S(1)}, u32[]{:S(2)}) copy-start(f32[2,64,128,256]{3,2,1,0:T(8,128)S(1)} %multiply_add_fusion) | copy-start | bytes 50331652

commit v2 on v1

--- a/solution.py
+++ b/solution.py
@@ -165,6 +165,25 @@
     return result
 
 
+def sending_order(chips):
+    return sorted(range(chips), key=lambda m: (-(m // 4), -(m % 2), -m))
+
+
+def landing_order(chip, chips):
+    ends = list(range(chips))
+    inside = [0, 1] + list(range(chips - 1, 1, -1))
+    place = lax.div(chip * 4, chips)
+    inner = lax.rem(lax.div(place + 1, 2), 2)
+    return [
+        (
+            flip(chip, a) + inner * (flip(chip, b) - flip(chip, a)),
+            a + inner * (b - a),
+            a,
+        )
+        for a, b in zip(ends, inside)
+    ]
+
+
 def fetch(source, target, sem):
     copy = pltpu.make_async_copy(source, target, sem)
     copy.start()
@@ -211,6 +230,12 @@
     numer[pl.ds(start, rows), :] = total
 
 
+def head_sums(q_head, k_head, n_head, my_stab, my_decay, my_weight):
+    denom = jnp.sum(q_head * (my_decay * n_head + my_weight * k_head), axis=-1, keepdims=True)
+    inner = jnp.sum(q_head * k_head, axis=-1, keepdims=True)
+    return inner, jnp.maximum(jnp.abs(denom), jnp.exp(-my_stab))
+
+
 def send_half(half, chip, core, chips, rows, source, dest, send, recv):
     me = chip * 2 + core
     return [
@@ -221,28 +246,29 @@
             send.at[half, m],
             recv.at[m, core],
         )
-        for m in range(chips - 1, 0, -1)
-    ]
-
-
-def gather_project(chip, core, chips, rows, source, dest, send, recv, weights, copies):
+        for m in sending_order(chips)
+        if m
+    ]
+
+
+def send_across(chip, core, rows, source, dest, send, recv):
     me = chip * 2 + core
+    dest[me] = source[pl.ds(pl.multiple_of(core * rows, rows), rows), :]
+    return push(
+        source.at[pl.ds(pl.multiple_of((1 - core) * rows, rows), rows)],
+        dest.at[me],
+        chip * 2 + 1 - core,
+        send.at[0, 0],
+        recv.at[0, core],
+    )
+
+
+def gather_project(chip, core, chips, rows, dest, recv, weights):
     partner = chip * 2 + 1 - core
     ncols = dest.shape[2]
-    copies.append(
-        push(
-            source.at[pl.ds(pl.multiple_of((1 - core) * rows, rows), rows)],
-            dest.at[me],
-            partner,
-            send.at[0, 0],
-            recv.at[0, core],
-        )
-    )
-    dest[me] = source[pl.ds(pl.multiple_of(core * rows, rows), rows), :]
     total = jnp.zeros((rows, 2 * ncols), jnp.float32)
-    for m in range(chips):
-        other = flip(chip, m)
-        if m == 0:
+    for other, m, at in landing_order(chip, chips):
+        if at == 0:
             arrived(dest.at[partner], recv.at[0, 1 - core])
         else:
             for c in range(2):
@@ -274,10 +300,11 @@
     key_buf,
     decay_buf,
     q_out,
-    inner_out,
-    den_out,
+    norm_out,
+    scale_out,
     gate_out,
     own_out,
+    proj_out,
     tok_buf,
     gain_buf,
     weights,
@@ -291,6 +318,7 @@
     send_buf,
     branch_buf,
     result_buf,
+    result_out,
     whole_buf,
     swap_buf,
     swap_out,
@@ -346,14 +374,12 @@
     def own_rows(ref, i):
         return ref.at[pl.ds(pl.multiple_of(i * 2 * ncols + core * ncols, ncols), ncols)]
 
-    def scale(gates, layer):
+    def scale(gates, layer, old_stab):
         in_gate = gates[:, :heads]
         forget = gates[:, heads : 2 * heads] + bias_buf[pl.ds(layer, 1), :]
         log_forget = jnp.minimum(forget, 0.0) - jnp.log1p(jnp.exp(-jnp.abs(forget)))
-        old_stab = stab_buf[layer].T
         next_stab = jnp.maximum(log_forget + old_stab, in_gate)
-        new_stab[layer] = next_stab.T
-        mine = lax.broadcasted_iota(jnp.int32, (batch, heads), 1) == chip
+        mine = lax.broadcasted_iota(jnp.int32, next_stab.shape, 1) == chip
 
         def pick(entry):
             return jnp.sum(jnp.where(mine, entry, 0.0), axis=-1, keepdims=True)
@@ -361,18 +387,15 @@
         my_stab = pick(next_stab)
         my_decay = jnp.exp(pick(log_forget + old_stab) - my_stab)
         my_weight = jnp.exp(pick(in_gate) - my_stab)
-        return my_stab, my_decay, my_weight
-
-    def finish_head(layer, q_head, k_head, my_stab, my_decay, my_weight):
-        n_head = jnp.concatenate([norm_buf[j, layer] for j in range(2)], axis=1)
-        denom = jnp.sum(
-            q_head * (my_decay * n_head + my_weight * k_head), axis=-1, keepdims=True
-        )
-        inner = jnp.sum(q_head * k_head, axis=-1, keepdims=True)
-        return inner, jnp.maximum(jnp.abs(denom), jnp.exp(-my_stab))
-
+        return next_stab, my_stab, my_decay, my_weight
+
+    gain_copy.wait()
     tok_copy.wait()
-    gain_copy.wait()
+    cell_copies = fetch_cell(0)
+    proj_copies = [fetch(w_proj.at[0], own_rows(proj_buf, 0), small_sem.at[6])]
+    wide_copies = [
+        fetch(names[i].at[1], own_rows(wide, i), wide_sem.at[i]) for i in range(4)
+    ]
     current = tok_buf[...].astype(jnp.float32)
     mean = jnp.sum(current * current, axis=-1, keepdims=True) * (1.0 / width)
     normed = (current * lax.rsqrt(mean + epsilon) * gain_buf[0:1, :]).astype(jnp.bfloat16)
@@ -389,8 +412,6 @@
     for copy in small:
         copy.wait()
     norm_copy.wait()
-    proj_copy = fetch(w_proj.at[0], own_rows(proj_buf, 0), small_sem.at[6])
-    cell_copies = fetch_cell(0)
     pl.semaphore_wait(barrier, n - 1)
     pair_copies = [
         push(pair_buf.at[core], pair_buf.at[core], partner, pair_send.at[0], pair_recv.at[0]),
@@ -402,26 +423,25 @@
     value = both[:, :ncols].astype(jnp.bfloat16).astype(jnp.float32)
     gate = jax.nn.sigmoid(both[:, ncols:].astype(jnp.bfloat16).astype(jnp.float32))
     gates = lax.dot_general(normed, gate_buf[0], NT, preferred_element_type=jnp.float32)
-    my_stab, my_decay, my_weight = scale(gates, 0)
+    next_stab, my_stab, my_decay, my_weight = scale(gates, 0, stab_buf[0].T)
+    new_stab[0] = next_stab.T
     new_norm[0] = my_decay * norm_buf[core, 0] + my_weight * key.astype(jnp.float32)
     weighted = my_weight * value
     wv_buf[0] = weighted
     decay_buf[0] = jnp.broadcast_to(my_decay, (batch, ncols))
     arrived(pair_buf.at[1 - core], pair_recv.at[0])
     arrived(norm_buf.at[1 - core], pair_recv.at[1])
-    proj_copy.wait()
-    pair_copies.append(
-        push(own_rows(proj_buf, 0), own_rows(proj_buf, 0), partner, pair_send.at[2], pair_recv.at[2])
-    )
     q_head = jnp.concatenate([pair_buf[j, 0] for j in range(2)], axis=1).astype(jnp.float32)
     k_head = jnp.concatenate([pair_buf[j, 1] for j in range(2)], axis=1).astype(jnp.float32)
     key_buf[0] = k_head
-    inner, den = finish_head(0, q_head, k_head, my_stab, my_decay, my_weight)
+    n_head = jnp.concatenate([norm_buf[j, 0] for j in range(2)], axis=1)
+    inner, den = head_sums(q_head, k_head, n_head, my_stab, my_decay, my_weight)
 
     branch_copies = []
     for h in range(2):
         for c in range(h * CELL_CHUNKS // 2, (h + 1) * CELL_CHUNKS // 2):
             cell_copies[c].wait()
+        for c in range(h * CELL_CHUNKS // 2, (h + 1) * CELL_CHUNKS // 2):
             queries = jnp.concatenate(
                 [pair_buf[j, 0, pl.ds(c * rows, rows), :] for j in range(2)], axis=1
             )
@@ -432,12 +452,12 @@
         branch_copies += send_half(
             h, chip, core, chips, half, send_buf, branch_buf, branch_send, branch_recv
         )
-    wide_copies = [
-        fetch(names[i].at[1], own_rows(wide, i), wide_sem.at[i]) for i in range(4)
-    ]
-    cell_copies = fetch_cell(1)
-    arrived(
-        proj_buf.at[pl.ds(pl.multiple_of((1 - core) * ncols, ncols), ncols)], pair_recv.at[2]
+    branch_copies.append(
+        send_across(chip, core, half, send_buf, branch_buf, branch_send, branch_recv)
+    )
+    proj_copies[0].wait()
+    pair_copies.append(
+        push(own_rows(proj_buf, 0), own_rows(proj_buf, 0), partner, pair_send.at[2], pair_recv.at[2])
     )
     wide_pushes = []
     for i in range(4):
@@ -451,33 +471,31 @@
                 pair_recv.at[3 + i],
             )
         )
-    summed = gather_project(
-        chip,
-        core,
-        chips,
-        half,
-        send_buf,
-        branch_buf,
-        branch_send,
-        branch_recv,
-        proj_buf,
-        branch_copies,
-    )
+    proj_copies.append(fetch(w_proj.at[1], own_rows(proj_out, 0), small_sem.at[7]))
+    cell_copies = fetch_cell(1)
+    arrived(
+        proj_buf.at[pl.ds(pl.multiple_of((1 - core) * ncols, ncols), ncols)], pair_recv.at[2]
+    )
+    summed = gather_project(chip, core, chips, half, branch_buf, branch_recv, proj_buf)
     my_rows = pl.ds(pl.multiple_of(core * half, half), half)
     my_cols = pl.ds(pl.multiple_of(chip * 2 * ncols, 2 * ncols), 2 * ncols)
     result = (tok_buf[my_rows, my_cols].astype(jnp.float32) + summed).astype(jnp.bfloat16)
     own_out[...] = result
-    result_buf[chip] = result
+    result_out[...] = result
     result_copies = [
         push(
+            result_out,
             result_buf.at[chip],
-            result_buf.at[chip],
-            flip(chip, m) * 2 + core,
+            flip(chip, m) * 2 + 1 - core,
             result_send.at[m],
             result_recv.at[m],
         )
-        for m in range(chips - 1, 0, -1)
-    ]
+        for m in sending_order(chips)
+    ]
+    proj_copies[1].wait()
+    pair_copies.append(
+        push(own_rows(proj_out, 0), own_rows(proj_out, 0), partner, pair_send.at[9], pair_recv.at[9])
+    )
 
     for i in range(4):
         arrived(
@@ -487,10 +505,8 @@
     total = jnp.zeros((half, 8 * ncols), jnp.float32)
     gates = jnp.zeros((half, 2 * heads), jnp.float32)
     square = jnp.zeros((half, 1), jnp.float32)
-    for m in range(chips):
-        other = flip(chip, m)
-        if m:
-            arrived(result_buf.at[other], result_recv.at[m])
+    for other, m, _ in landing_order(chip, chips):
+        arrived(result_buf.at[other], result_recv.at[m])
         cols = pl.ds(pl.multiple_of(other * 2 * ncols, 2 * ncols), 2 * ncols)
         block = result_buf[other].astype(jnp.float32)
         square = square + jnp.sum(block * block, axis=-1, keepdims=True)
@@ -502,73 +518,82 @@
             block, gate_buf[1, :, cols], NT, preferred_element_type=jnp.float32
         )
     root = lax.rsqrt(square * (1.0 / width) + epsilon)
+    old_stab = jnp.where(core == 0, stab_buf[1].T[half:], stab_buf[1].T[:half])
+    scalars = scale(gates * root, 1, old_stab)
+    gates_buf[1 - core] = jnp.concatenate(
+        scalars + (jnp.zeros((half, ncols - heads - 3), jnp.float32),), axis=1
+    )
     total = total * root
     query = total[:, : 2 * ncols].astype(jnp.bfloat16)
     key = (total[:, 2 * ncols : 4 * ncols] * dh ** (-0.5)).astype(jnp.bfloat16)
     whole_buf[...] = total[:, 4 * ncols :].astype(jnp.bfloat16)
-    for target, side in ((swap_buf.at[core], core), (swap_out, 1 - core)):
+    for target, side in ((swap_out, 1 - core), (swap_buf.at[1 - core], core)):
         target[:, : 2 * ncols] = query
         target[:, 2 * ncols : 4 * ncols] = key
         for i in range(2):
             target[:, (4 + i) * ncols : (5 + i) * ncols] = whole_buf[
                 :, pl.ds(pl.multiple_of(i * 2 * ncols + side * ncols, ncols), ncols)
             ]
-    gates_buf[core] = jnp.concatenate(
-        [gates * root, jnp.zeros((half, ncols - 2 * heads), jnp.float32)], axis=1
-    )
     pair_copies += [
-        push(swap_out, swap_buf.at[core], partner, pair_send.at[7], pair_recv.at[7]),
-        push(gates_buf.at[core], gates_buf.at[core], partner, pair_send.at[8], pair_recv.at[8]),
-    ]
+        push(swap_out, swap_buf.at[1 - core], partner, pair_send.at[7], pair_recv.at[7]),
+        push(
+            gates_buf.at[1 - core],
+            gates_buf.at[1 - core],
+            partner,
+            pair_send.at[8],
+            pair_recv.at[8],
+        ),
+    ]
+    for j in range(2):
+        norm_out[j] = norm_buf[j, 1]
     for copy in branch_copies + wide_pushes + result_copies:
         copy.wait_send()
     for copy in cell_copies:
         copy.wait()
-    arrived(swap_buf.at[1 - core], pair_recv.at[7])
-    arrived(gates_buf.at[1 - core], pair_recv.at[8])
+    arrived(
+        proj_out.at[pl.ds(pl.multiple_of((1 - core) * ncols, ncols), ncols)], pair_recv.at[9]
+    )
+    arrived(swap_buf.at[core], pair_recv.at[7])
+    arrived(gates_buf.at[core], pair_recv.at[8])
 
     def both_halves(part):
         return jnp.concatenate([swap_buf[j, :, part] for j in range(2)], axis=0)
 
-    gates = jnp.concatenate([gates_buf[j] for j in range(2)], axis=0)
-    my_stab, my_decay, my_weight = scale(gates, 1)
-    queries = both_halves(slice(0, 2 * ncols))
-    q_out[...] = queries
-    q_head = queries.astype(jnp.float32)
-    k_head = both_halves(slice(2 * ncols, 4 * ncols)).astype(jnp.float32)
-    key_buf[1] = k_head
+    scalars = jnp.concatenate([gates_buf[j] for j in range(2)], axis=0)
+    scale_out[...] = scalars
+    new_stab[1] = scalars[:, :heads].T
+    my_decay = scalars[:, heads + 1 : heads + 2]
+    my_weight = scalars[:, heads + 2 : heads + 3]
+    q_out[...] = both_halves(slice(0, 2 * ncols))
+    key_buf[1] = both_halves(slice(2 * ncols, 4 * ncols)).astype(jnp.float32)
+    wv_buf[1] = my_weight * both_halves(slice(4 * ncols, 5 * ncols)).astype(jnp.float32)
+    decay_buf[1] = jnp.broadcast_to(my_decay, (batch, ncols))
+    gate_out[...] = both_halves(slice(5 * ncols, 6 * ncols))
     key = both_halves(pl.ds(pl.multiple_of((2 + core) * ncols, ncols), ncols))
     new_norm[1] = my_decay * norm_buf[core, 1] + my_weight * key.astype(jnp.float32)
-    weighted = my_weight * both_halves(slice(4 * ncols, 5 * ncols)).astype(jnp.float32)
-    wv_buf[1] = weighted
-    decay_buf[1] = jnp.broadcast_to(my_decay, (batch, ncols))
-    gate_out[...] = jax.nn.sigmoid(both_halves(slice(5 * ncols, 6 * ncols)).astype(jnp.float32))
-    inner, den = finish_head(1, q_head, k_head, my_stab, my_decay, my_weight)
-    inner_out[...] = weighted * inner
-    den_out[...] = jnp.broadcast_to(den, (batch, ncols))
     for copy in pair_copies:
         copy.wait_send()
 
 
 def last_kernel(
     n,
+    heads,
     cell_buf,
     queries,
-    decay,
-    inner,
-    den,
-    gate,
+    keys,
+    norms,
+    weighted,
+    scalars,
+    outgate,
     own,
+    proj_buf,
     _,
-    w_proj,
     mixed,
-    proj_buf,
     send_buf,
     branch_buf,
     swap_buf,
     swap_out,
     numer_buf,
-    proj_sem,
     pair_send,
     pair_recv,
     branch_send,
@@ -584,58 +609,41 @@
     chip = lax.div(me, 2)
     partner = chip * 2 + 1 - core
     barrier = greet_all(n, me)
-    own_part = proj_buf.at[pl.ds(pl.multiple_of(core * ncols, ncols), ncols)]
-    proj_copy = fetch(w_proj.at[last], own_part, proj_sem)
+    for c in range(CELL_CHUNKS):
+        read_rows(
+            lambda b: cell_buf[last, b],
+            queries[pl.ds(c * rows, rows), :],
+            numer_buf,
+            c * rows,
+            rows,
+        )
+    q_head = queries[...].astype(jnp.float32)
+    n_head = jnp.concatenate([norms[j] for j in range(2)], axis=1)
+    my_stab, my_decay, my_weight = (scalars[:, heads + i : heads + i + 1] for i in range(3))
+    inner, den = head_sums(q_head, keys[last], n_head, my_stab, my_decay, my_weight)
+    numer = my_decay * numer_buf[...] + weighted[last] * inner
+    gate = jax.nn.sigmoid(outgate[...].astype(jnp.float32))
+    send_buf[...] = (gate * (numer / den)).astype(jnp.bfloat16)
+    pl.semaphore_wait(barrier, n - 1)
     copies = []
     for h in range(2):
-        for c in range(h * CELL_CHUNKS // 2, (h + 1) * CELL_CHUNKS // 2):
-            read_rows(
-                lambda b: cell_buf[last, b],
-                queries[pl.ds(c * rows, rows), :],
-                numer_buf,
-                c * rows,
-                rows,
-            )
-        part = slice(h * half, (h + 1) * half)
-        numer = decay[last, part, :] * numer_buf[part, :] + inner[part, :]
-        send_buf[part, :] = (gate[part, :] * (numer / den[part, :])).astype(jnp.bfloat16)
-        if h == 0:
-            pl.semaphore_wait(barrier, n - 1)
         copies += send_half(
             h, chip, core, chips, half, send_buf, branch_buf, branch_send, branch_recv
         )
-    proj_copy.wait()
-    pair_copies = [push(own_part, own_part, partner, pair_send.at[0], pair_recv.at[0])]
-    arrived(
-        proj_buf.at[pl.ds(pl.multiple_of((1 - core) * ncols, ncols), ncols)], pair_recv.at[0]
-    )
-    summed = gather_project(
-        chip,
-        core,
-        chips,
-        half,
-        send_buf,
-        branch_buf,
-        branch_send,
-        branch_recv,
-        proj_buf,
-        copies,
-    )
+    copies.append(send_across(chip, core, half, send_buf, branch_buf, branch_send, branch_recv))
+    summed = gather_project(chip, core, chips, half, branch_buf, branch_recv, proj_buf)
     result = (own[...].astype(jnp.float32) + summed).astype(jnp.bfloat16)
     swap_buf[...] = result
     swap_out[core] = swap_buf[:, pl.ds(pl.multiple_of((1 - core) * ncols, ncols), ncols)]
-    pair_copies.append(
-        push(swap_out.at[core], swap_out.at[2 + core], partner, pair_send.at[1], pair_recv.at[1])
-    )
+    swap_copy = push(swap_out.at[core], swap_out.at[2 + core], partner, pair_send, pair_recv)
     mixed[pl.ds(pl.multiple_of(core * half, half), half), :] = swap_buf[
         :, pl.ds(pl.multiple_of(core * ncols, ncols), ncols)
     ]
     for copy in copies:
         copy.wait_send()
-    arrived(swap_out.at[3 - core], pair_recv.at[1])
+    arrived(swap_out.at[3 - core], pair_recv)
     mixed[pl.ds(pl.multiple_of((1 - core) * half, half), half), :] = swap_out[3 - core]
-    for copy in pair_copies:
-        copy.wait_send()
+    swap_copy.wait_send()
 
 
 def fused_body(n, *args):
@@ -652,8 +660,7 @@
     vmem = pl.BlockSpec(memory_space=pltpu.VMEM)
     hbm = pl.BlockSpec(memory_space=pltpu.HBM)
     dma = pltpu.SemaphoreType.DMA
-    rows = jax.ShapeDtypeStruct((batch, ncols), f32)
-    held, new_norm, new_stab, weighted, keys, decay, queries, inner, den, gate, own = pl.pallas_call(
+    held, new_norm, new_stab, weighted, keys, decay, *rest = pl.pallas_call(
         functools.partial(cells_kernel, n),
         out_shape=(
             pltpu.VMEM(cell.shape, f32),
@@ -663,13 +670,14 @@
             jax.ShapeDtypeStruct((layers, batch, dh), f32),
             jax.ShapeDtypeStruct((layers, batch, ncols), f32),
             jax.ShapeDtypeStruct((batch, dh), bf16),
-            rows,
-            rows,
-            rows,
+            jax.ShapeDtypeStruct((2, batch, ncols), f32),
+            jax.ShapeDtypeStruct((batch, ncols), f32),
+            jax.ShapeDtypeStruct((batch, ncols), bf16),
             jax.ShapeDtypeStruct((half, dh), bf16),
+            jax.ShapeDtypeStruct((2 * ncols, width), bf16),
         ),
         in_specs=[hbm] * len(args),
-        out_specs=(vmem,) * 11,
+        out_specs=(vmem,) * 12,
         scratch_shapes=[
             pltpu.VMEM(tokens.shape, bf16),
             pltpu.VMEM(norm_gain.shape, f32),
@@ -684,17 +692,18 @@
             pltpu.VMEM((batch, ncols), bf16),
             pltpu.VMEM((n, half, ncols), bf16),
             pltpu.VMEM((chips, half, 2 * ncols), bf16),
+            pltpu.VMEM((half, 2 * ncols), bf16),
             pltpu.VMEM((half, 4 * ncols), bf16),
             pltpu.VMEM((2, half, 6 * ncols), bf16),
             pltpu.VMEM((half, 6 * ncols), bf16),
             pltpu.VMEM((2, half, ncols), f32),
             pltpu.VMEM((batch, ncols), f32),
-            dma((7,)),
+            dma((8,)),
             dma((4,)),
             dma((4,)),
             dma((layers, CELL_CHUNKS)),
-            dma((9,)),
-            dma((9,)),
+            dma((10,)),
+            dma((10,)),
             dma((2, chips)),
             dma((chips, 2)),
             dma((chips,)),
@@ -708,21 +717,20 @@
     new_cell = (
         decay[:, :, :1, None] * held + weighted[:, :, :, None] * keys[:, :, None, :]
     )
+    queries, norms, scalars, outgate, own, proj = rest
     mixed = pl.pallas_call(
-        functools.partial(last_kernel, n),
+        functools.partial(last_kernel, n, stab.shape[1]),
         out_shape=jax.ShapeDtypeStruct((batch, ncols), bf16),
-        in_specs=[vmem] * 8 + [hbm],
+        in_specs=[vmem] * 10,
         out_specs=vmem,
         scratch_shapes=[
-            pltpu.VMEM((2 * ncols, width), bf16),
             pltpu.VMEM((batch, ncols), bf16),
             pltpu.VMEM((n, half, ncols), bf16),
             pltpu.VMEM((half, 2 * ncols), bf16),
             pltpu.VMEM((4, half, ncols), bf16),
             pltpu.VMEM((batch, ncols), f32),
             dma,
-            dma((2,)),
-            dma((2,)),
+            dma,
             dma((2, chips)),
             dma((chips, 2)),
         ],
@@ -733,7 +741,18 @@
             flops=5 * 10**10, bytes_accessed=10**6, transcendentals=0
         ),
         name="last",
-    )(held, queries, decay, inner, den, gate, own, new_cell[0, 0, :8, :128], args[8])
+    )(
+        held,
+        queries,
+        keys,
+        norms,
+        weighted,
+        scalars,
+        outgate,
+        own,
+        proj,
+        new_cell[0, 0, :8, :128],
+    )
     mixed, new_norm, new_stab = write_small(mixed, new_norm, new_stab)
     return mixed, new_cell, new_norm, jnp.swapaxes(new_stab, 1, 2)
 

time: 37.7 us -> 33.9 us (0.90)
  Pallas kernels: 33.7 us -> 30 us
    pallas_call x1, Pallas kernels: 23.9 us -> 20.7 us  [fused_body(): pl.pallas_call(functools.partial(cells_kernel, n), out_shape=(pltpu.VMEM(...]
    pallas_call x1, Pallas kernels: 9.22 us -> 8.59 us  [fused_body(): pl.pallas_call(functools.partial(last_kernel, n, stab.shape[1]), out_shap...]
where the time goes in v2:
time: 33.9 us; the launch traced here: 33.8 us
  Pallas kernels  30 us (88%)
  other arithmetic  3.03 us (9%)
  between operations  0.69 us (2%)
    pallas_call x1, Pallas kernels, fused_body(): pl.pallas_call(functools.partial(cells_kernel, n), out_shape=(pltpu.VMEM(...  20.7 us
    pallas_call x1, Pallas kernels, fused_body(): pl.pallas_call(functools.partial(last_kernel, n, stab.shape[1]), out_shap...  8.59 us
    add x1, other arithmetic, fused_body(): decay[:, :, :1, None] * held + weighted[:, :, :, None] * keys[:, :, None, :]  3.03 us

profile of v2, /device:TPU:0, one launch (start us, length us, event | category | flops | bytes accessed | tf_op | source)
XLA Modules:
  0.0 33.8 jit_solution(4857622552776112489)
XLA Ops:
  0.6 20.7 %cells.1 = (f32[2,64,128,256]{3,2,1,0:T(8,128)S(1)}, f32[2,64,128]{2,1,0:T(8,128)S(1)}, f32[2,8,64]{2,1,0:T(8,128)S(1)}, f32[2,64,128]{2,1,0:T(8,128)S(1)}, f32[...) custom-call(bf16[64,2048]{1,0:T(8,128)(2,1)} %tokens.1, ...), custom_call_target="tpu_custom_call" | custom-call | tf_op jit(solution)/shard_map/cells/pallas_call | solution.py:663
  21.4 0.1 slice_reduce_fusion
  21.4 3.0 %multiply_add_fusion = f32[2,64,128,256]{3,2,1,0:T(8,128)S(1)} fusion(f32[2,64,128,256]{3,2,1,0:T(8,128)S(1)} %get-tuple-element.19.cell_buf, f32[2,64,256]{2,1,0:T(8,128)S(1)} %get-tuple-element.21.keys, f32[2,64,128]{2,1,0:T(8,128)S(1)} %get-tuple-element.23.weighted, f32[2,64]{1,0:T(2,128)S(1)} %slice_reduce_fusion), kind=kLoop, calls=%fused_computation | loop fusion | flops 12582912 | bytes 33751552 | tf_op jit(solution)/shard_map/add | solution.py:718
  24.5 0.0 copy-start
  24.5 8.6 %last.1.refs_0_ = bf16[64,128]{1,0:T(8,128)(2,1)S(1)} custom-call(f32[2,64,128,256]{3,2,1,0:T(8,128)S(1)} %get-tuple-element.19.cell_buf, bf16[64,256]{1,0:T(8,128)(2,1)S(1)} %get-tuple-element.20.queries, f32[2,64,256]{2,1,0:T(8,128)S(1)} %get-tuple-element.21.keys, f32[2,64,128]{2,1,0:T(8,128)S(1)} %get-tuple-element.22.norms, ...), custom_call_target="tpu_custom_call" | custom-call | flops 49999998976 | bytes 1000000 | tf_op jit(solution)/shard_map/last/pallas_call | solution.py:721
  33.1 0.0 copy-done
  33.1 0.7 %write.1 = (bf16[64,128]{1,0:T(8,128)(2,1)}, f32[2,64,128]{2,1,0:T(8,128)}, f32[2,8,64]{2,1,0:T(8,128)}) custom-call(bf16[64,128]{1,0:T(8,128)(2,1)S(1)} %last.1.refs_0_, f32[2,64,128]{2,1,0:T(8,128)S(1)} %get-tuple-element.29.refs_1_, f32[2,8,64]{2,1,0:T(8,128)S(1)} %get-tuple-element.30.refs_2_), custom_call_target="tpu_custom_call" | custom-call | tf_op jit(solution)/shard_map/write/pallas_call | solution.py:773
  (1 shorter events, 0.0 us)
Async XLA Ops:
  24.5 8.6 %copy-start = (f32[2,64,128,256]{3,2,1,0:T(8,128)}, f32[2,64,128,256]{3,2,1,0:T(8,128)S(1)}, u32[]{:S(2)}) copy-start(f32[2,64,128,256]{3,2,1,0:T(8,128)S(1)} %multiply_add_fusion) | copy-start | bytes 50331652

commit v3 on v2

--- a/solution.py
+++ b/solution.py
@@ -169,6 +169,22 @@
     return sorted(range(chips), key=lambda m: (-(m // 4), -(m % 2), -m))
 
 
+def first_to_zero(chip, chips):
+    masks = [m for m in sending_order(chips) if m]
+    pairs = []
+    for at, m in enumerate(masks):
+        same = 1 - lax.div((chip - m) * (chip - m) + chips * chips - 1, chips * chips)
+        if at == 0:
+            zero = 1 - lax.div(chip * chip + chips * chips - 1, chips * chips)
+            pairs.append((zero * flip(chip, m), chip + zero * m))
+        else:
+            top = masks[0]
+            pairs.append(
+                (flip(chip, m) + same * (flip(chip, top) - flip(chip, m)), m + same * (top - m))
+            )
+    return pairs
+
+
 def landing_order(chip, chips):
     ends = list(range(chips))
     inside = [0, 1] + list(range(chips - 1, 1, -1))
@@ -230,10 +246,16 @@
     numer[pl.ds(start, rows), :] = total
 
 
-def head_sums(q_head, k_head, n_head, my_stab, my_decay, my_weight):
+def update_rows(cells, decay, weighted, keys):
+    columns = weighted.T
+    for r in range(weighted.shape[0]):
+        row = slice(r, r + 1)
+        cells[r] = decay[row] * cells[r] + columns[:, row] * keys[row]
+
+
+def bound(q_head, k_head, n_head, my_stab, my_decay, my_weight):
     denom = jnp.sum(q_head * (my_decay * n_head + my_weight * k_head), axis=-1, keepdims=True)
-    inner = jnp.sum(q_head * k_head, axis=-1, keepdims=True)
-    return inner, jnp.maximum(jnp.abs(denom), jnp.exp(-my_stab))
+    return jnp.maximum(jnp.abs(denom), jnp.exp(-my_stab))
 
 
 def send_half(half, chip, core, chips, rows, source, dest, send, recv):
@@ -296,9 +318,8 @@
     cell_buf,
     new_norm,
     new_stab,
-    wv_buf,
-    key_buf,
-    decay_buf,
+    one_out,
+    key_out,
     q_out,
     norm_out,
     scale_out,
@@ -390,12 +411,8 @@
         return next_stab, my_stab, my_decay, my_weight
 
     gain_copy.wait()
+    cell_copies = fetch_cell(0)
     tok_copy.wait()
-    cell_copies = fetch_cell(0)
-    proj_copies = [fetch(w_proj.at[0], own_rows(proj_buf, 0), small_sem.at[6])]
-    wide_copies = [
-        fetch(names[i].at[1], own_rows(wide, i), wide_sem.at[i]) for i in range(4)
-    ]
     current = tok_buf[...].astype(jnp.float32)
     mean = jnp.sum(current * current, axis=-1, keepdims=True) * (1.0 / width)
     normed = (current * lax.rsqrt(mean + epsilon) * gain_buf[0:1, :]).astype(jnp.bfloat16)
@@ -427,20 +444,24 @@
     new_stab[0] = next_stab.T
     new_norm[0] = my_decay * norm_buf[core, 0] + my_weight * key.astype(jnp.float32)
     weighted = my_weight * value
-    wv_buf[0] = weighted
-    decay_buf[0] = jnp.broadcast_to(my_decay, (batch, ncols))
     arrived(pair_buf.at[1 - core], pair_recv.at[0])
     arrived(norm_buf.at[1 - core], pair_recv.at[1])
     q_head = jnp.concatenate([pair_buf[j, 0] for j in range(2)], axis=1).astype(jnp.float32)
     k_head = jnp.concatenate([pair_buf[j, 1] for j in range(2)], axis=1).astype(jnp.float32)
-    key_buf[0] = k_head
     n_head = jnp.concatenate([norm_buf[j, 0] for j in range(2)], axis=1)
-    inner, den = head_sums(q_head, k_head, n_head, my_stab, my_decay, my_weight)
+    inner = jnp.sum(q_head * k_head, axis=-1, keepdims=True)
+    den = bound(q_head, k_head, n_head, my_stab, my_decay, my_weight)
 
     branch_copies = []
     for h in range(2):
         for c in range(h * CELL_CHUNKS // 2, (h + 1) * CELL_CHUNKS // 2):
             cell_copies[c].wait()
+        if h == 1:
+            proj_copies = [fetch(w_proj.at[0], own_rows(proj_buf, 0), small_sem.at[6])]
+            wide_copies = [
+                fetch(names[i].at[1], own_rows(wide, i), wide_sem.at[i]) for i in range(4)
+            ]
+            proj_copies.append(fetch(w_proj.at[1], own_rows(proj_out, 0), small_sem.at[7]))
         for c in range(h * CELL_CHUNKS // 2, (h + 1) * CELL_CHUNKS // 2):
             queries = jnp.concatenate(
                 [pair_buf[j, 0, pl.ds(c * rows, rows), :] for j in range(2)], axis=1
@@ -471,8 +492,11 @@
                 pair_recv.at[3 + i],
             )
         )
-    proj_copies.append(fetch(w_proj.at[1], own_rows(proj_out, 0), small_sem.at[7]))
     cell_copies = fetch_cell(1)
+    proj_copies[1].wait()
+    pair_copies.append(
+        push(own_rows(proj_out, 0), own_rows(proj_out, 0), partner, pair_send.at[9], pair_recv.at[9])
+    )
     arrived(
         proj_buf.at[pl.ds(pl.multiple_of((1 - core) * ncols, ncols), ncols)], pair_recv.at[2]
     )
@@ -492,11 +516,9 @@
         )
         for m in sending_order(chips)
     ]
-    proj_copies[1].wait()
-    pair_copies.append(
-        push(own_rows(proj_out, 0), own_rows(proj_out, 0), partner, pair_send.at[9], pair_recv.at[9])
-    )
-
+
+    update_rows(cell_buf.at[0], my_decay, weighted, k_head)
+    one_out[...] = jnp.ones_like(one_out)
     for i in range(4):
         arrived(
             wide.at[pl.ds(pl.multiple_of(i * 2 * ncols + (1 - core) * ncols, ncols), ncols)],
@@ -546,15 +568,27 @@
     ]
     for j in range(2):
         norm_out[j] = norm_buf[j, 1]
+    for copy in cell_copies:
+        copy.wait()
+
+    def update_half(side):
+        scalars = gates_buf[side]
+        my_decay = scalars[:, heads + 1 : heads + 2]
+        my_weight = scalars[:, heads + 2 : heads + 3]
+        keys = swap_buf[side, :, 2 * ncols : 4 * ncols].astype(jnp.float32)
+        value = swap_buf[side, :, 4 * ncols : 5 * ncols].astype(jnp.float32)
+        cells = cell_buf.at[1, pl.ds(side * half, half)]
+        update_rows(cells, my_decay, my_weight * value, keys)
+
+    update_half(1 - core)
     for copy in branch_copies + wide_pushes + result_copies:
         copy.wait_send()
-    for copy in cell_copies:
-        copy.wait()
     arrived(
         proj_out.at[pl.ds(pl.multiple_of((1 - core) * ncols, ncols), ncols)], pair_recv.at[9]
     )
     arrived(swap_buf.at[core], pair_recv.at[7])
     arrived(gates_buf.at[core], pair_recv.at[8])
+    update_half(core)
 
     def both_halves(part):
         return jnp.concatenate([swap_buf[j, :, part] for j in range(2)], axis=0)
@@ -565,9 +599,7 @@
     my_decay = scalars[:, heads + 1 : heads + 2]
     my_weight = scalars[:, heads + 2 : heads + 3]
     q_out[...] = both_halves(slice(0, 2 * ncols))
-    key_buf[1] = both_halves(slice(2 * ncols, 4 * ncols)).astype(jnp.float32)
-    wv_buf[1] = my_weight * both_halves(slice(4 * ncols, 5 * ncols)).astype(jnp.float32)
-    decay_buf[1] = jnp.broadcast_to(my_decay, (batch, ncols))
+    key_out[...] = both_halves(slice(2 * ncols, 4 * ncols))
     gate_out[...] = both_halves(slice(5 * ncols, 6 * ncols))
     key = both_halves(pl.ds(pl.multiple_of((2 + core) * ncols, ncols), ncols))
     new_norm[1] = my_decay * norm_buf[core, 1] + my_weight * key.astype(jnp.float32)
@@ -582,7 +614,6 @@
     queries,
     keys,
     norms,
-    weighted,
     scalars,
     outgate,
     own,
@@ -620,16 +651,21 @@
     q_head = queries[...].astype(jnp.float32)
     n_head = jnp.concatenate([norms[j] for j in range(2)], axis=1)
     my_stab, my_decay, my_weight = (scalars[:, heads + i : heads + i + 1] for i in range(3))
-    inner, den = head_sums(q_head, keys[last], n_head, my_stab, my_decay, my_weight)
-    numer = my_decay * numer_buf[...] + weighted[last] * inner
+    den = bound(q_head, keys[...].astype(jnp.float32), n_head, my_stab, my_decay, my_weight)
     gate = jax.nn.sigmoid(outgate[...].astype(jnp.float32))
-    send_buf[...] = (gate * (numer / den)).astype(jnp.bfloat16)
+    send_buf[...] = (gate * (numer_buf[...] / den)).astype(jnp.bfloat16)
     pl.semaphore_wait(barrier, n - 1)
-    copies = []
-    for h in range(2):
-        copies += send_half(
-            h, chip, core, chips, half, send_buf, branch_buf, branch_send, branch_recv
-        )
+    copies = [
+        push(
+            send_buf.at[pl.ds(h * half, half)],
+            branch_buf.at[me],
+            target * 2 + h,
+            branch_send.at[h, m],
+            branch_recv.at[m, core],
+        )
+        for target, m in first_to_zero(chip, chips)
+        for h in range(2)
+    ]
     copies.append(send_across(chip, core, half, send_buf, branch_buf, branch_send, branch_recv))
     summed = gather_project(chip, core, chips, half, branch_buf, branch_recv, proj_buf)
     result = (own[...].astype(jnp.float32) + summed).astype(jnp.bfloat16)
@@ -660,15 +696,14 @@
     vmem = pl.BlockSpec(memory_space=pltpu.VMEM)
     hbm = pl.BlockSpec(memory_space=pltpu.HBM)
     dma = pltpu.SemaphoreType.DMA
-    held, new_norm, new_stab, weighted, keys, decay, *rest = pl.pallas_call(
+    held, new_norm, new_stab, one, *rest = pl.pallas_call(
         functools.partial(cells_kernel, n),
         out_shape=(
             pltpu.VMEM(cell.shape, f32),
             jax.ShapeDtypeStruct(norm_vec.shape, f32),
             jax.ShapeDtypeStruct(stab.shape, f32),
-            jax.ShapeDtypeStruct((layers, batch, ncols), f32),
-            jax.ShapeDtypeStruct((layers, batch, dh), f32),
-            jax.ShapeDtypeStruct((layers, batch, ncols), f32),
+            jax.ShapeDtypeStruct((1, dh), f32),
+            jax.ShapeDtypeStruct((batch, dh), bf16),
             jax.ShapeDtypeStruct((batch, dh), bf16),
             jax.ShapeDtypeStruct((2, batch, ncols), f32),
             jax.ShapeDtypeStruct((batch, ncols), f32),
@@ -677,7 +712,7 @@
             jax.ShapeDtypeStruct((2 * ncols, width), bf16),
         ),
         in_specs=[hbm] * len(args),
-        out_specs=(vmem,) * 12,
+        out_specs=(vmem,) * 11,
         scratch_shapes=[
             pltpu.VMEM(tokens.shape, bf16),
             pltpu.VMEM(norm_gain.shape, f32),
@@ -714,14 +749,12 @@
         ),
         name="cells",
     )(*args)
-    new_cell = (
-        decay[:, :, :1, None] * held + weighted[:, :, :, None] * keys[:, :, None, :]
-    )
-    queries, norms, scalars, outgate, own, proj = rest
+    new_cell = held * one[0]
+    keys, queries, norms, scalars, outgate, own, proj = rest
     mixed = pl.pallas_call(
         functools.partial(last_kernel, n, stab.shape[1]),
         out_shape=jax.ShapeDtypeStruct((batch, ncols), bf16),
-        in_specs=[vmem] * 10,
+        in_specs=[vmem] * 9,
         out_specs=vmem,
         scratch_shapes=[
             pltpu.VMEM((batch, ncols), bf16),
@@ -746,7 +779,6 @@
         queries,
         keys,
         norms,
-        weighted,
         scalars,
         outgate,
         own,

time: 33.9 us -> 33 us (0.973)
  other arithmetic: 3.03 us -> 1.47 us
  Pallas kernels: 30 us -> 30.7 us
    add x1 -> x0, other arithmetic: 3.03 us -> none  [fused_body(): decay[:, :, :1, None] * held + weighted[:, :, :, None] * keys[:, :, None, :]]
    mul x0 -> x1, other arithmetic: none -> 1.47 us  [fused_body(): new_cell = held * one[0]]
    pallas_call x1, Pallas kernels: 20.7 us -> 22 us  [fused_body(): pl.pallas_call(functools.partial(cells_kernel, n), out_shape=(pltpu.VMEM(...]
    pallas_call x1, Pallas kernels: 8.59 us -> 8.04 us  [fused_body(): pl.pallas_call(functools.partial(last_kernel, n, stab.shape[1]), out_shap...]
where the time goes in v3:
time: 33 us; the launch traced here: 32.9 us
  Pallas kernels  30.7 us (93%)
  other arithmetic  1.47 us (4%)
  between operations  0.68 us (2%)
    pallas_call x1, Pallas kernels, fused_body(): pl.pallas_call(functools.partial(cells_kernel, n), out_shape=(pltpu.VMEM(...  22 us
    pallas_call x1, Pallas kernels, fused_body(): pl.pallas_call(functools.partial(last_kernel, n, stab.shape[1]), out_shap...  8.04 us
    mul x1, other arithmetic, fused_body(): new_cell = held * one[0]  1.47 us
    pallas_call x1, Pallas kernels, write_small(): pl.pallas_call(write_kernel, out_shape=[jax.ShapeDtypeStruct(x.shape, x.d...  0.67 us

profile of v3, /device:TPU:0, one launch (start us, length us, event | category | flops | bytes accessed | tf_op | source)
XLA Modules:
  0.0 32.9 jit_solution(11209151039628937066)
XLA Ops:
  0.6 22.0 %cells.1 = (f32[2,64,128,256]{3,2,1,0:T(8,128)S(1)}, f32[2,64,128]{2,1,0:T(8,128)S(1)}, f32[2,8,64]{2,1,0:T(8,128)S(1)}, f32[1,256]{1,0:T(1,128)S(1)}, bf16[64,2...) custom-call(bf16[64,2048]{1,0:T(8,128)(2,1)} %tokens.1, ...), custom_call_target="tpu_custom_call" | custom-call | tf_op jit(solution)/shard_map/cells/pallas_call | solution.py:699
  22.7 1.5 %broadcast_multiply_fusion = f32[2,64,128,256]{3,2,1,0:T(8,128)S(1)} fusion(f32[2,64,128,256]{3,2,1,0:T(8,128)S(1)} %get-tuple-element.18.cell_buf, f32[256]{0:T(256)S(1)} %bitcast.6), kind=kLoop, calls=%fused_computation | loop fusion | flops 4194304 | bytes 33555456 | tf_op jit(solution)/shard_map/mul | solution.py:752
  24.1 0.0 copy-start
  24.2 8.0 %last.1.refs_0_ = bf16[64,128]{1,0:T(8,128)(2,1)S(1)} custom-call(f32[2,64,128,256]{3,2,1,0:T(8,128)S(1)} %get-tuple-element.18.cell_buf, bf16[64,256]{1,0:T(8,128)(2,1)S(1)} %get-tuple-element.19.queries, bf16[64,256]{1,0:T(8,128)(2,1)S(1)} %get-tuple-element.20.keys, f32[2,64,128]{2,1,0:T(8,128)S(1)} %get-tuple-element.21.norms, ...), custom_call_target="tpu_custom_call" | custom-call | flops 49999998976 | bytes 1000000 | tf_op jit(solution)/shard_map/last/pallas_call | solution.py:754
  32.2 0.0 copy-done
  32.2 0.7 %write.1 = (bf16[64,128]{1,0:T(8,128)(2,1)}, f32[2,64,128]{2,1,0:T(8,128)}, f32[2,8,64]{2,1,0:T(8,128)}) custom-call(bf16[64,128]{1,0:T(8,128)(2,1)S(1)} %last.1.refs_0_, f32[2,64,128]{2,1,0:T(8,128)S(1)} %get-tuple-element.27.refs_1_, f32[2,8,64]{2,1,0:T(8,128)S(1)} %get-tuple-element.28.refs_2_), custom_call_target="tpu_custom_call" | custom-call | tf_op jit(solution)/shard_map/write/pallas_call | solution.py:805
  (1 shorter events, 0.0 us)
Async XLA Ops:
  24.1 8.1 %copy-start = (f32[2,64,128,256]{3,2,1,0:T(8,128)}, f32[2,64,128,256]{3,2,1,0:T(8,128)S(1)}, u32[]{:S(2)}) copy-start(f32[2,64,128,256]{3,2,1,0:T(8,128)S(1)} %broadcast_multiply_fusion) | copy-start | bytes 50331652
